TPU v7x, 256 devices: a whole 4x4x8 slice. The times are simulated.
256 devices in a mesh: rep: 2 (over z_hi), fs: 16 (over z_lo, y), tp: 8 (over x, core).
Axes of the slice: x: 4, y: 4, z: 8 (z_hi: 2, z_lo: 4; z = z_hi * 4 + z_lo), core: 2. Of those that a mesh axis runs over, the one named last changes fastest.
Arguments:
- stream: bfloat16 [32768, 2048], P(('rep', 'fs', 'tp')), may hold values from -6 to 6
- gain_before: float32 [2048], replicated, may hold values from 0.1 to 1.9
- gain_after: float32 [2048], replicated, may hold values from 0.1 to 1.9
- proj_gate: bfloat16 [2048, 3584], P('fs', 'tp'), may hold values from -0.125 to 0.125
- proj_lift: bfloat16 [2048, 3584], P('fs', 'tp'), may hold values from -0.125 to 0.125
- proj_down: bfloat16 [3584, 2048], P('tp', 'fs'), may hold values from -0.09375 to 0.09375
- mixer_gain: float32 [2048], replicated, may hold values from 0.1 to 1.9
- mixer_u: bfloat16 [2048, 2048], P('fs', 'tp'), may hold values from -0.125 to 0.125
- mixer_v: bfloat16 [2048, 2048], P('fs', 'tp'), may hold values from -1 to 1
- layer_gain: float32 [2048], P('tp'), may hold values from 0.1 to 1.9
- layer_shift: float32 [2048], P('tp'), may hold values from -3 to 3
- spatial: bfloat16 [16, 128, 128], P('tp'), may hold values from -0.5 to 0.5
- spatial_shift: float32 [16, 128], P('tp'), may hold values from 0.2 to 2
- mixer_down: bfloat16 [2048, 2048], P('tp', 'fs'), may hold values from -0.125 to 0.125
Outputs:
- result: bfloat16 [32768, 2048], P(('rep', 'fs', 'tp'))
All inputs are finite; a program needn't handle non-finite values.
Results may differ from a plain program's by a relative error of at most 0.017.
Values may be sent and summed in bfloat16 or wider, within the bound.
A program may use at most 128 MiB of HBM per device.

v0:
```python
import jax
import jax.numpy as jnp
from jax import lax
from jax.sharding import PartitionSpec as P

GROUP_DIM = 128
SPAN = 128
A = 2048


norm_epsilon = 1e-06
layer_epsilon = 1e-05


def sent_to_all(value, axis):
    copies = jnp.broadcast_to(value, (lax.axis_size(axis), *value.shape))
    return lax.all_to_all(copies, axis, split_axis=0, concat_axis=0, tiled=True)


def laid_out(tiles, dim):
    lengths = list(tiles.shape[1:])
    lengths[dim] *= tiles.shape[0]
    return jnp.moveaxis(tiles, 0, dim).reshape(lengths)


def gathered_copies(value, axis, dim):
    tiles = sent_to_all(value, axis)
    return laid_out(tiles, dim)


def side_by_side(arrays, axis, dim, along):
    ends, at = ([], 0)
    for a in arrays[:-1]:
        at += a.shape[along]
        ends.append(at)
    both = jnp.concatenate(arrays, axis=along)
    return tuple(jnp.split(lax.all_gather(both, axis, axis=dim, tiled=True), ends, axis=along))


def norm_rows(row_block, scale_gain):
    widened = row_block.astype(jnp.float32)
    factor = lax.rsqrt(jnp.mean(widened * widened, axis=1, keepdims=True) + norm_epsilon)
    return (widened * factor * scale_gain).astype(jnp.bfloat16)


def gathered_norm(stream_rows, scale_gain):
    gathered = lax.all_gather(stream_rows, "tp", axis=0, tiled=True)
    return norm_rows(gathered, scale_gain)


def pair_adder(normed, pieces):
    return (
        jnp.dot(normed, pieces[0], preferred_element_type=jnp.float32),
        jnp.dot(normed, pieces[1], preferred_element_type=jnp.float32),
    )


def activate(gate_vals, lift_vals):
    return (jax.nn.silu(gate_vals) * lift_vals).astype(jnp.bfloat16)


def rows_project(columns_here, weight_shard):
    weight_cols = gathered_copies(weight_shard, "fs", 1)
    weight_whole = lax.all_gather(weight_cols, "tp", axis=0, tiled=True)
    own_tokens = lax.all_to_all(columns_here, "tp", split_axis=0, concat_axis=1, tiled=True)
    width = columns_here.shape[1]
    running = jnp.zeros((own_tokens.shape[0], weight_whole.shape[1]), jnp.float32)
    for member in range(lax.axis_size("tp")):
        partial_value = jnp.dot(
            own_tokens[:, member * width : (member + 1) * width],
            weight_whole[member * width : (member + 1) * width],
            preferred_element_type=jnp.float32,
        )
        running = running + partial_value.astype(jnp.bfloat16).astype(jnp.float32)
    return running


def half_kept(stream_rows, scale_gain, gate_whole, lift_whole, proj_down):
    normed = gathered_norm(stream_rows, scale_gain)
    gate_vals = jnp.dot(normed, gate_whole, preferred_element_type=jnp.float32)
    lift_vals = jnp.dot(normed, lift_whole, preferred_element_type=jnp.float32)
    hidden = activate(gate_vals, lift_vals)
    summed = rows_project(hidden, proj_down)
    return (stream_rows.astype(jnp.float32) + 0.5 * summed).astype(jnp.bfloat16)


def token_mixer(
    stream_rows,
    mixer_gain,
    mixer_u,
    mixer_v,
    layer_gain,
    layer_shift,
    spatial,
    spatial_shift,
    mixer_down,
):
    gathered = lax.all_gather(stream_rows, "tp", axis=0, tiled=True)
    normed = norm_rows(gathered, mixer_gain)
    seq_tokens = normed.shape[0]
    u_vals, v_vals = pair_adder(normed, side_by_side((mixer_u, mixer_v), "fs", 0, 1))
    lifted = jax.nn.gelu(v_vals)
    moments = lax.psum((jnp.sum(lifted, axis=1), jnp.sum(lifted * lifted, axis=1)), "tp")
    centre = moments[0] / A
    spread = moments[1] / A - centre * centre
    normed_v = (
        (lifted - centre[:, None]) * lax.rsqrt(spread[:, None] + layer_epsilon) * layer_gain
        + layer_shift
    ).astype(jnp.bfloat16)
    groups_here = spatial.shape[0]
    blocked = normed_v.reshape(seq_tokens // SPAN, SPAN, groups_here, GROUP_DIM)
    causal = jnp.tril(jnp.ones((SPAN, SPAN), dtype=bool))
    masked = jnp.where(causal[None], spatial, jnp.zeros((), jnp.bfloat16))
    mixed_v = jnp.einsum("gts,bsgd->btgd", masked, blocked, preferred_element_type=jnp.float32)
    mixed_v = mixed_v + spatial_shift.T[None, :, :, None]
    gated = (jax.nn.gelu(u_vals) * mixed_v.reshape(seq_tokens, groups_here * GROUP_DIM)).astype(
        jnp.bfloat16
    )
    summed = rows_project(gated, mixer_down)
    return (stream_rows.astype(jnp.float32) + summed).astype(jnp.bfloat16)


def body(
    stream,
    gain_before,
    gain_after,
    proj_gate,
    proj_lift,
    proj_down,
    mixer_gain,
    mixer_u,
    mixer_v,
    layer_gain,
    layer_shift,
    spatial,
    spatial_shift,
    mixer_down,
):
    gate_whole, lift_whole = side_by_side((proj_gate, proj_lift), "fs", 0, 1)
    first = half_kept(stream, gain_before, gate_whole, lift_whole, proj_down)
    second = token_mixer(
        first,
        mixer_gain,
        mixer_u,
        mixer_v,
        layer_gain,
        layer_shift,
        spatial,
        spatial_shift,
        mixer_down,
    )
    result = half_kept(second, gain_after, gate_whole, lift_whole, proj_down)
    return result


def solution(mesh):
    placed = (
        P(("rep", "fs", "tp"), None),
        P(),
        P(),
        P("fs", "tp"),
        P("fs", "tp"),
        P("tp", "fs"),
        P(),
        P("fs", "tp"),
        P("fs", "tp"),
        P("tp"),
        P("tp"),
        P("tp", None, None),
        P("tp", None),
        P("tp", "fs"),
    )
    return jax.shard_map(
        body, mesh=mesh, in_specs=placed, out_specs=P(("rep", "fs", "tp"), None), check_vma=False
    )
```

profile of v0, /device:TPU:1, one launch (start us, length us, event | category | flops | bytes accessed | tf_op | source)
XLA Modules:
  0.0 495.1 jit_solution(2137628182025998506)
XLA Ops:
  6.5 0.7 all-gather.8.cloned.1.call-update
  7.3 1.7 pad_maximum_fusion
  9.0 1.2 broadcast_in_dim.14
  10.3 51.8 %all_to_all.68 = bf16[16,448,128]{2,1,0:T(8,128)(2,1)S(1)} all-to-all(bf16[16,448,128]{2,1,0:T(8,128)(2,1)S(1)} %broadcast_in_dim.14), channel_id=1, replica_groups=mesh['rep'=2,'fs'=16,'tp'=8] {'fs'}, dimensions={0} | all-to-all | bytes 3670016 | tf_op jit(solution)/shard_map/all_to_all | solution.py:17
  62.1 1.5 copy_bitcast_fusion
  63.7 3.1 fusion
  66.8 58.1 %all-gather.10.cloned.1.call-done = bf16[2048,896]{0,1:T(8,128)(2,1)} async-done(((bf16[128,896]{0,1:T(8,128)(2,1)}), bf16[2048,896]{0,1:T(8,128)(2,1)}) %all-gather.10.cloned.1.call-update) | async-done | bytes 3670032 | tf_op jit(solution)/shard_map/all_gather | solution.py:37
  124.9 5.1 %fusion.80 = f32[1024,448]{0,1:T(8,128)S(1)} fusion(bf16[2048,896]{0,1:T(8,128)(2,1)} %all-gather.10.cloned.1.call-done, bf16[1024,2048]{1,0:T(8,128)(2,1)} %all-gather.8.cloned.1.call-done, f32[2048]{0:T(1024)S(1)} %copy-done.16, f32[1024]{0:T(1024)S(1)} %add_rsqrt_fusion.3), kind=kOutput, calls=%fused_computation.113 | convolution fusion | flops 1887436800 | bytes 7876608 | tf_op jit(solution)/shard_map/dot_general | solution.py:81
  130.0 2.5 fusion.91
  132.7 34.0 %all_to_all.69 = bf16[8,128,448]{1,2,0:T(8,128)(2,1)S(1)} all-to-all(bf16[8,128,448]{1,2,0:T(8,128)(2,1)S(1)} %bitcast.46), channel_id=1, replica_groups=mesh['rep'=2,'fs'=16,'tp'=8] {'tp'}, dimensions={0} | all-to-all | bytes 1835008 | tf_op jit(solution)/shard_map/all_to_all | solution.py:65
  166.8 54.7 %all-gather.12.cloned.1.call-done = bf16[3584,2048]{1,0:T(8,128)(2,1)} async-done(((bf16[448,2048]{1,0:T(8,128)(2,1)}), bf16[3584,2048]{1,0:T(8,128)(2,1)}) %all-gather.12.cloned.1.call-update) | async-done | bytes 14680080 | tf_op jit(solution)/shard_map/all_gather | solution.py:64
  221.4 2.1 fusion.61
  223.5 2.4 fusion.60
  225.9 2.6 fusion.58
  228.5 2.0 fusion.56
  230.5 0.5 fusion.54
  231.0 0.5 fusion.52
  231.5 0.5 fusion.50
  232.0 1.3 fusion.48
  233.4 0.7 pad_maximum_fusion.1
  234.4 32.1 %all_to_all.70 = bf16[16,256,128]{1,2,0:T(8,128)(2,1)} all-to-all(bf16[16,256,128]{1,2,0:T(8,128)(2,1)S(1)} %broadcast_in_dim.21), channel_id=1, replica_groups=mesh['rep'=2,'fs'=16,'tp'=8] {'fs'}, dimensions={0} | all-to-all | bytes 2097152 | tf_op jit(solution)/shard_map/all_to_all | solution.py:17
  266.6 3.1 fusion.3
  269.7 70.9 %all-gather.16.cloned.1.call-done = bf16[2048,512]{1,0:T(8,128)(2,1)} async-done(((bf16[128,512]{1,0:T(8,128)(2,1)}), bf16[2048,512]{1,0:T(8,128)(2,1)}) %all-gather.16.cloned.1.call-update) | async-done | bytes 2097168 | tf_op jit(solution)/shard_map/all_gather | solution.py:37
  340.6 4.1 fusion.169
  344.7 22.8 %all-reduce = (f32[1024]{0:T(1024)S(1)}, f32[1024]{0:T(1024)S(1)}) all-reduce(f32[1024]{0:T(1024)S(1)} %get-tuple-element.6, f32[1024]{0:T(1024)S(1)} %get-tuple-element.5), channel_id=1, replica_groups=mesh['rep'=2,'fs'=16,'tp'=8] {'tp'}, use_global_device_ids=true, to_apply=%region_5.6 | all-reduce | flops 2048 | bytes 16384 | tf_op jit(solution)/shard_map/psum | solution.py:103
  368.4 0.6 copy.41
  369.0 4.0 fusion.117
  373.1 1.0 copy.42
  374.1 4.1 all-to-all-start.2
  378.2 34.6 %all-gather.18.cloned.1.call-done = bf16[2048,2048]{0,1:T(8,128)(2,1)} async-done(((bf16[256,2048]{0,1:T(8,128)(2,1)}), bf16[2048,2048]{0,1:T(8,128)(2,1)}) %all-gather.18.cloned.1.call-update) | async-done | bytes 8388624 | tf_op jit(solution)/shard_map/all_gather | solution.py:64
  412.8 1.9 fusion.43
  414.7 2.1 fusion.42
  416.8 1.7 fusion.40
  418.5 0.5 fusion.38
  419.0 0.5 fusion.36
  419.5 0.5 fusion.34
  420.0 0.5 fusion.32
  420.5 1.3 fusion.30
  421.9 34.6 %all-gather.20.cloned.1.call-done = bf16[1024,2048]{1,0:T(8,128)(2,1)} async-done(((bf16[128,2048]{1,0:T(8,128)(2,1)}), bf16[1024,2048]{1,0:T(8,128)(2,1)}) %all-gather.20.cloned.1.call-update) | async-done | bytes 4194320 | tf_op jit(solution)/shard_map/all_gather | solution.py:47
  456.5 3.2 fusion.6
  459.9 4.0 fusion.78
  464.0 2.6 fusion.94
  466.8 16.7 %all_to_all.71 = bf16[8,128,448]{1,2,0:T(8,128)(2,1)S(1)} all-to-all(bf16[8,128,448]{1,2,0:T(8,128)(2,1)S(1)} %bitcast.47), channel_id=1, replica_groups=mesh['rep'=2,'fs'=16,'tp'=8] {'tp'}, dimensions={0} | all-to-all | bytes 1835008 | tf_op jit(solution)/shard_map/all_to_all | solution.py:65
  483.5 0.5 fusion.26
  484.0 0.5 fusion.25
  484.5 0.5 fusion.23
  486.4 0.5 fusion.15
  487.0 1.3 fusion.13
  (78 shorter events, 3.6 us)
Async XLA Ops:
  6.5 57.1 %all-gather.8.cloned.1.call-start = ((), (), s32[]{:S(2)}) async-start(), calls=%async_computation.5 | async-start | bytes 4718592 | tf_op jit(solution)/shard_map/all_gather | solution.py:47
  7.3 117.6 %all-gather.10.cloned.1.call-start = ((), (), s32[]{:S(2)}) async-start(), calls=%async_computation.6 | async-start | bytes 3899392 | tf_op jit(solution)/shard_map/all_gather | solution.py:37
  9.0 212.4 %all-gather.12.cloned.1.call-start = ((), (), s32[]{:S(2)}) async-start(), calls=%async_computation.7 | async-start | bytes 16515072 | tf_op jit(solution)/shard_map/all_gather | solution.py:64
  62.1 62.8 %copy-start.16 = (f32[2048]{0:T(1024)S(1)}, f32[2048]{0:T(1024)}, u32[]{:S(2)}) copy-start(f32[2048]{0:T(1024)} %param.15) | copy-start | bytes 24580
  63.6 203.0 %all-gather.14.cloned.1.call-start = ((), (), s32[]{:S(2)}) async-start(), calls=%async_computation.8 | async-start | bytes 4718592 | tf_op jit(solution)/shard_map/all_gather | solution.py:98
  124.9 5.1 %copy-start.4 = (bf16[1024,2048]{1,0:T(8,128)(2,1)S(1)}, bf16[1024,2048]{1,0:T(8,128)(2,1)}, u32[]{:S(2)}) copy-start(bf16[1024,2048]{1,0:T(8,128)(2,1)} %all-gather.8.cloned.1.call-done) | copy-start | bytes 12582916
  124.9 5.1 %copy-start.14 = (bf16[2048,896]{0,1:T(8,128)(2,1)S(1)}, bf16[2048,896]{0,1:T(8,128)(2,1)}, u32[]{:S(2)}) copy-start(bf16[2048,896]{0,1:T(8,128)(2,1)} %all-gather.10.cloned.1.call-done) | copy-start | bytes 11010052
  221.4 9.1 %copy-start = (bf16[3584,2048]{1,0:T(8,128)(2,1)S(1)}, bf16[3584,2048]{1,0:T(8,128)(2,1)}, u32[]{:S(2)}) copy-start(bf16[3584,2048]{1,0:T(8,128)(2,1)} %all-gather.12.cloned.1.call-done) | copy-start | bytes 44040196
  231.0 1.0 copy-start.6
  231.5 1.9 copy-start.9
  231.5 1.9 copy-start.10
  231.5 2.7 copy-start.8
  233.4 107.2 %all-gather.16.cloned.1.call-start = ((), (), s32[]{:S(2)}) async-start(), calls=%async_computation.9 | async-start | bytes 2228224 | tf_op jit(solution)/shard_map/all_gather | solution.py:37
  234.1 178.7 %all-gather.18.cloned.1.call-start = ((), (), s32[]{:S(2)}) async-start(), calls=%async_computation.10 | async-start | bytes 9437184 | tf_op jit(solution)/shard_map/all_gather | solution.py:64
  234.3 106.3 %copy-start.17 = (f32[2048]{0:T(1024)S(1)}, f32[2048]{0:T(1024)}, u32[]{:S(2)}) copy-start(f32[2048]{0:T(1024)} %param.20) | copy-start | bytes 24580
  269.6 97.9 %copy-start.11 = (f32[256]{0:T(256)S(1)}, f32[256]{0:T(256)}, u32[]{:S(2)}) copy-start(f32[256]{0:T(256)} %param.24) | copy-start | bytes 3076
  269.7 97.9 %copy-start.12 = (f32[256]{0:T(256)S(1)}, f32[256]{0:T(256)}, u32[]{:S(2)}) copy-start(f32[256]{0:T(256)} %param.23) | copy-start | bytes 3076
  269.7 98.4 %copy-start.7 = (bf16[2,128,128]{2,1,0:T(8,128)(2,1)S(1)}, bf16[2,128,128]{2,1,0:T(8,128)(2,1)}, u32[]{:S(2)}) copy-start(bf16[2,128,128]{2,1,0:T(8,128)(2,1)} %param.25) | copy-start | bytes 196612
  269.7 98.3 %copy-start.13 = (f32[2,128]{1,0:T(2,128)S(1)}, f32[2,128]{1,0:T(2,128)}, u32[]{:S(2)}) copy-start(f32[2,128]{1,0:T(2,128)} %param.26) | copy-start | bytes 3076
  374.1 38.7 %all-to-all-start.2 = ((bf16[8,128,256]{1,2,0:T(8,128)(2,1)}), bf16[8,128,256]{1,2,0:T(8,128)(2,1)S(1)}, u32[]{:S(2)}, u32[]{:S(2)}) async-start(bf16[8,128,256]{1,2,0:T(8,128)(2,1)} %copy.42), calls=%async_computation.2 | async-start | bytes 1048576 | tf_op jit(solution)/shard_map/all_to_all | solution.py:65
  378.2 78.3 %all-gather.20.cloned.1.call-start = ((), (), s32[]{:S(2)}) async-start(), calls=%async_computation.11 | async-start | bytes 4718592 | tf_op jit(solution)/shard_map/all_gather | solution.py:47
  412.8 5.7 %copy-start.1 = (bf16[2048,2048]{0,1:T(8,128)(2,1)S(1)}, bf16[2048,2048]{0,1:T(8,128)(2,1)}, u32[]{:S(2)}) copy-start(bf16[2048,2048]{0,1:T(8,128)(2,1)} %all-gather.18.cloned.1.call-done) | copy-start | bytes 25165828
  419.0 1.5 copy-start.2
  420.5 39.2 %copy-start.18 = (f32[2048]{0:T(1024)S(1)}, f32[2048]{0:T(1024)}, u32[]{:S(2)}) copy-start(f32[2048]{0:T(1024)} %param.16) | copy-start | bytes 24580
  456.5 3.4 copy-start.5
  459.9 4.0 copy-start.15
  459.9 23.5 %slice-start = ((s8[14680064]{0:T(1024)(128)(4,1)}), s8[4194304]{0:T(1024)(128)(4,1)S(1)}, s32[]{:S(2)}) async-start(s8[14680064]{0:T(1024)(128)(4,1)} %bitcast.43), calls=%async_computation.12 | async-start | bytes 8388608
  459.9 23.5 %slice-start.1 = ((s8[14680064]{0:T(1024)(128)(4,1)}), s8[4194304]{0:T(1024)(128)(4,1)S(1)}, s32[]{:S(2)}) async-start(s8[14680064]{0:T(1024)(128)(4,1)} %bitcast.43), calls=%async_computation.13 | async-start | bytes 8388608
  463.9 19.5 %slice-start.2 = ((s8[14680064]{0:T(1024)(128)(4,1)}), s8[4194304]{0:T(1024)(128)(4,1)S(1)}, s32[]{:S(2)}) async-start(s8[14680064]{0:T(1024)(128)(4,1)} %bitcast.43), calls=%async_computation.14 | async-start | bytes 8388608
  464.0 19.5 %slice-start.3 = ((s8[14680064]{0:T(1024)(128)(4,1)}), s8[2097152]{0:T(1024)(128)(4,1)S(1)}, s32[]{:S(2)}) async-start(s8[14680064]{0:T(1024)(128)(4,1)} %bitcast.43), calls=%async_computation.15 | async-start | bytes 4194304
  485.9 1.0 copy-start.3
Sparse Core Ops, SparseCore 0:
  9.2 38.7 all-gather.7
  49.7 75.1 all-gather.9
  126.7 94.6 all-gather.11
  233.5 33.0 all-gather.13
  268.2 72.3 all-gather.15
  342.2 70.5 all-gather.17
  422.0 34.4 all-gather.19
where the time goes:
time: 496 us; the launch traced here: 495 us
  waiting for transfers between devices  254 us (51%)
  blocking collectives  157 us (32%)
  matrix products  48 us (10%)
  between operations  14 us (3%)
  other arithmetic  12.1 us (2%)
  local copies, waits for them, and re-layouts  5.48 us (1%)
    all_gather x2, waiting for transfers between devices, side_by_side(): lax.all_gather(both, axis, axis=dim, tiled=True)  129 us
    all_gather x2, waiting for transfers between devices, rows_project(): weight_whole = lax.all_gather(weight_cols, 'tp', axis=0, tiled=True)  89.3 us
    all_to_all x2, blocking collectives, sent_to_all(): return lax.all_to_all(copies, axis, split_axis=0, concat_axis=0, tiled=True)  83.9 us
    all_to_all x2, blocking collectives, rows_project(): lax.all_to_all(columns_here, 'tp', split_axis=0, concat_axis=1, tiled=True)  50.8 us
    all_gather x2, waiting for transfers between devices, gathered_norm(): gathered = lax.all_gather(stream_rows, 'tp', axis=0, tiled=True)  34.6 us
    dot_general x24, matrix products, rows_project(): jnp.dot(own_tokens[:, member * width:(member + 1) * width], weight_whole[...  25.3 us
    psum x1, blocking collectives, token_mixer(): lax.psum((jnp.sum(lifted, axis=1), jnp.sum(lifted * lifted, axis=1)), 'tp')  22.8 us
  transfers between devices with their start and end apart: 8, of which 5 were waited for; matrix products, arithmetic and copies ran while one was open for 6% of the time, Pallas kernels for 0%

commit v1 on v0

v1 whole, which is shorter than its diff:
```python
import jax
import jax.numpy as jnp
from jax import lax
from jax.experimental import pallas as pl
from jax.experimental.pallas import tpu as pltpu
from jax.sharding import PartitionSpec as P

MESH = pl.DeviceIdType.MESH
F32 = jnp.float32
BF16 = jnp.bfloat16
A = 2048
norm_epsilon = 1e-06
layer_epsilon = 1e-05
L, R = 0, 1
GL, DN, UV, MD = 0, 1, 2, 3
W_ROWS = (128, 448, 128, 256)
CH = 2
CROWS = 128 // CH
STEP = 16


def silu(v):
    return v / (1.0 + jnp.exp(-v))


def gelu(v):
    return 0.5 * v * (1.0 + jnp.tanh(0.7978845608028654 * (v + 0.044715 * (v * v * v))))


def dot(a, b):
    return jnp.dot(a, b, preferred_element_type=F32)


def widx(w, s, part, phase, i):
    return (((w * 2 + s) * 2 + part) * 2 + phase) * 4 + i


def kernel(
    stream, gain_b, gain_a, p_gate, p_lift, p_down, m_gain, m_u, m_v, l_gain, l_shift, spat, s_shift, m_down,
    out,
    wgl, wd, wuv, wmd, msp, sp2, prm,
    xs, po, ps, pc, pr, acc, hid, hid2, gu, lf, res, sto, sti, colm,
    w_send, w_recv, sw_send, sw_recv, ag_send, ag_recv, rs_send, rs_recv, st_send, st_recv,
):
    rep, fs, tp = lax.axis_index("rep"), lax.axis_index("fs"), lax.axis_index("tp")
    x, c = tp // 2, tp % 2
    zl, y = fs // 4, fs % 4
    z8 = rep * 4 + zl

    def dev(dx, dy, dz, dc):
        return (dz // 4, (dz % 4) * 4 + dy, dx * 2 + dc)

    sib = dev(x, y, z8, 1 - c)
    xo = (x + 1 + 2 * ((x + c) % 2)) % 4
    xt = (x + 1 + 2 * ((x + c + 1) % 2)) % 4
    partner = dev(xo, y, z8, c)
    y_plus, y_minus = dev(x, (y + 1) % 4, z8, c), dev(x, (y + 3) % 4, z8, c)
    z_plus, z_minus = dev(x, y, (z8 + 1) % 8, c), dev(x, y, (z8 + 7) % 8, c)
    swap_to = dev((x + 2) % 4, y, z8, c)
    weights = (wgl, wd, wuv, wmd)

    barrier = pltpu.get_barrier_semaphore()
    greeted = (
        sib, partner, dev(xo, y, z8, 1 - c), dev(xt, y, z8, 0), dev(xt, y, z8, 1),
        y_plus, y_minus, z_plus, z_minus, swap_to,
    )
    for other in greeted:
        pl.semaphore_signal(barrier, inc=1, device_id=other, device_id_type=MESH)

    sent = []

    def remote(src, dst, ssem, rsem, to):
        return pltpu.make_async_remote_copy(
            src_ref=src, dst_ref=dst, send_sem=ssem, recv_sem=rsem, device_id=to, device_id_type=MESH
        )

    def start(copy):
        copy.start()
        sent.append(copy)

    def region(w, s, part, phase, pos, sub):
        n = W_ROWS[w] // 2
        r0 = part * n
        if sub is not None:
            n //= 2
            r0 += sub * n
        rows = pl.ds(r0, n)
        ref = weights[w]
        if phase == 0:
            return ref.at[s, zl, pos, rows] if part == 0 else ref.at[s, pos, y, rows]
        return ref.at[s, pos, :, rows] if part == 0 else ref.at[s, :, pos, rows]

    def ring(part, phase):
        if part == phase:
            return y, y_plus, y_minus
        return zl, z_plus, z_minus

    def w_start(w, s, part, phase, i):
        me, plus, minus = ring(part, phase)
        pos = (me, me, (me + 3) % 4, (me + 1) % 4)[i]
        block = region(w, s, part, phase, pos, (None, None, 0, 1)[i])
        j = widx(w, s, part, phase, i)
        start(remote(block, block, w_send.at[j], w_recv.at[j], (plus, minus, plus, minus)[i]))

    def w_wait(w, s, part, phase, i):
        me, plus, minus = ring(part, phase)
        pos = ((me + 3) % 4, (me + 1) % 4, (me + 2) % 4, (me + 2) % 4)[i]
        block = region(w, s, part, phase, pos, (None, None, 0, 1)[i])
        j = widx(w, s, part, phase, i)
        remote(block, block, w_send.at[j], w_recv.at[j], plus).wait_recv()

    def p1(w, s):
        for part in (0, 1):
            for i in (0, 1):
                w_start(w, s, part, 0, i)

    def forward(w, s, phase):
        for part in (0, 1):
            for i in (0, 1):
                w_wait(w, s, part, phase, i)
                w_start(w, s, part, phase, i + 2)

    def p2(w, s):
        forward(w, s, 0)

    def p3(w, s):
        for part in (0, 1):
            w_wait(w, s, part, 0, 2)
            w_wait(w, s, part, 0, 3)
            for i in (0, 1):
                w_start(w, s, part, 1, i)

    def p4(w, s):
        forward(w, s, 1)

    def p5(w, s):
        for part in (0, 1):
            w_wait(w, s, part, 1, 2)
            w_wait(w, s, part, 1, 3)

    def swap(w):
        ref = weights[w]
        return remote(ref.at[0, zl, y], ref.at[1, zl, y], sw_send.at[w], sw_recv.at[w], swap_to)

    def ag_own(r, ch):
        rows = pl.ds(ch * CROWS, CROWS)
        j = r * 3 * CH + ch
        return (
            remote(xs.at[r, L, 0, rows], xs.at[r, R, 0, rows], ag_send.at[j], ag_recv.at[j], partner),
            remote(xs.at[r, L, 0, rows], xs.at[r, L, 1, rows], ag_send.at[j + CH], ag_recv.at[j + CH], sib),
        )

    def ag_fwd(r, ch):
        rows = pl.ds(ch * CROWS, CROWS)
        j = r * 3 * CH + 2 * CH + ch
        return remote(xs.at[r, R, 0, rows], xs.at[r, R, 1, rows], ag_send.at[j], ag_recv.at[j], sib)

    def ag_recv_partner(r, ch):
        rows = pl.ds(ch * CROWS, CROWS)
        j = r * 3 * CH + ch
        return remote(xs.at[r, R, 0, rows], xs.at[r, R, 0, rows], ag_send.at[j], ag_recv.at[j], partner)

    def ag_recv_sib(r, ch):
        rows = pl.ds(ch * CROWS, CROWS)
        j = r * 3 * CH + CH + ch
        return remote(xs.at[r, L, 1, rows], xs.at[r, L, 1, rows], ag_send.at[j], ag_recv.at[j], sib)

    def ag_recv_fwd(r, ch):
        rows = pl.ds(ch * CROWS, CROWS)
        j = r * 3 * CH + 2 * CH + ch
        return remote(xs.at[r, R, 1, rows], xs.at[r, R, 1, rows], ag_send.at[j], ag_recv.at[j], sib)

    def rs_d2d(r, b):
        j = r * (2 + CH) + b
        return remote(po.at[r, b], ps.at[r, b], rs_send.at[j], rs_recv.at[j], sib)

    def rs_ici(r, ch):
        rows = pl.ds(ch * CROWS, CROWS)
        j = r * (2 + CH) + 2 + ch
        return remote(pc.at[r, rows], pr.at[r, rows], rs_send.at[j], rs_recv.at[j], partner)

    def normed(rows, gain):
        factor = lax.rsqrt(jnp.mean(rows * rows, axis=1, keepdims=True) + norm_epsilon)
        return (rows * factor * gain[...]).astype(BF16)

    def ag_send_chunk(r, ch):
        for copy in ag_own(r, ch):
            start(copy)

    def ag_wait_left(r):
        for ch in range(CH):
            ag_recv_sib(r, ch).wait_recv()

    def ag_relay(r):
        for ch in range(CH):
            ag_recv_partner(r, ch).wait_recv()
            start(ag_fwd(r, ch))

    def ag_wait_right(r):
        for ch in range(CH):
            ag_recv_fwd(r, ch).wait_recv()

    wgl[0, zl, y] = jnp.concatenate(
        [
            piece
            for j in range(3)
            for piece in (p_gate[:, j * 128 : (j + 1) * 128], p_lift[:, j * 128 : (j + 1) * 128])
        ]
        + [p_gate[:, 384:448], p_lift[:, 384:448]],
        axis=1,
    )

    @pl.loop(0, 128 // STEP)
    def _(i):
        rows = pl.ds(i * STEP, STEP)
        old = stream[rows, :]
        res[rows, :] = old
        xs[0, L, 0, rows, :] = normed(old.astype(F32), gain_b)

    wd[0, zl, y] = p_down[...]
    wuv[0, zl, y] = jnp.concatenate([m_u[...], m_v[...]], axis=1)
    wmd[0, zl, y] = m_down[...]
    prm[0] = jnp.concatenate([l_gain[...], l_shift[...], s_shift[...], jnp.zeros((2, 128), F32)], axis=0)
    sp2[0] = spat[...]

    pl.semaphore_wait(barrier, len(greeted))

    p1(GL, 0)
    start(swap(GL))
    for ch in range(CH):
        ag_send_chunk(0, ch)
    p1(DN, 0)
    start(swap(DN))
    p1(UV, 0)
    start(swap(UV))
    p1(MD, 0)
    start(swap(MD))
    swap_prm = remote(prm.at[0], prm.at[1], sw_send.at[4], sw_recv.at[4], swap_to)
    swap_sp = remote(sp2.at[0], sp2.at[1], sw_send.at[5], sw_recv.at[5], swap_to)
    start(swap_prm)
    start(swap_sp)

    def batch_x(r, b):
        return xs[r, b].reshape(256, 2048)

    def up_slot(r, b, s):
        @pl.loop(0, 3)
        def _(j):
            cols = pl.ds(pl.multiple_of(j * 256, 256), 256)
            o = dot(batch_x(r, b), wgl[s, :, :, :, cols].reshape(2048, 256))
            to = pl.ds(pl.multiple_of(s * 384 + j * 128, 128), 128)
            hid[b, :, to] = (silu(o[:, :128]) * o[:, 128:]).astype(BF16)

    def up_tail(r, b):
        w = jnp.concatenate([wgl[s, :, :, :, 768:896].reshape(2048, 128) for s in (0, 1)], axis=1)
        o = dot(batch_x(r, b), w)
        t0, t1 = o[:, :128], o[:, 128:]
        low = lax.broadcasted_iota(jnp.int32, (256, 128), 1) < 64
        gate = jnp.where(low, t0, pltpu.roll(t1, 64, axis=1))
        lift = jnp.where(low, pltpu.roll(t0, 64, axis=1), t1)
        hid[b, :, 768:896] = (silu(gate) * lift).astype(BF16)

    def up(r, b):
        @pl.loop(0, 2)
        def _(s):
            up_slot(r, b, s)

        up_tail(r, b)

    def wd_cols(zz, yy):
        return jnp.concatenate(
            [wd[0, zz, yy, 0:384], wd[1, zz, yy, 0:384], wd[0, zz, yy, 384:448], wd[1, zz, yy, 384:448]], axis=0
        )

    def wmd_cols(zz, yy):
        return jnp.concatenate([wmd[0, zz, yy], wmd[1, zz, yy]], axis=0)

    def down(r, b, lhs, columns_of):
        @pl.loop(0, 8)
        def _(n):
            zz, yy = n // 2, (n % 2) * 2
            rhs = jnp.concatenate([columns_of(zz, yy), columns_of(zz, yy + 1)], axis=1)
            o = dot(lhs[b], rhs)
            cols = pl.ds(pl.multiple_of(n * 256, 256), 256)
            acc[b, :, cols] = o[:128]
            po[r, b, :, cols] = o[128:].astype(BF16)

        start(rs_d2d(r, b))

    def rs_right(r):
        rs_d2d(r, R).wait_recv()
        for ch in range(CH):

            @pl.loop(0, CROWS // STEP)
            def _(i):
                rows = pl.ds(ch * CROWS + i * STEP, STEP)
                pc[r, rows, :] = (acc[R, rows, :] + ps[r, R, rows, :].astype(F32)).astype(BF16)

            start(rs_ici(r, ch))

    def rs_left(r, coefficient, gain):
        rs_d2d(r, L).wait_recv()
        for ch in range(CH):
            rs_ici(r, ch).wait_recv()

            @pl.loop(0, CROWS // STEP)
            def _(i):
                rows = pl.ds(ch * CROWS + i * STEP, STEP)
                delta = acc[L, rows, :] + ps[r, L, rows, :].astype(F32) + pr[r, rows, :].astype(F32)
                new = (res[rows, :].astype(F32) + coefficient * delta).astype(BF16)
                if gain is None:
                    out[rows, :] = new
                else:
                    res[rows, :] = new
                    xs[r + 1, L, 0, rows, :] = normed(new.astype(F32), gain)

            if gain is not None:
                ag_send_chunk(r + 1, ch)

    def mixer_up(b):
        @pl.loop(0, 2)
        def _(s):
            to = pl.ds(pl.multiple_of(s * 256, 256), 256)
            gu[b, :, to] = gelu(dot(batch_x(1, b), wuv[s, :, :, :, 0:256].reshape(2048, 256)))
            lf[b, :, to] = gelu(dot(batch_x(1, b), wuv[s, :, :, :, 256:512].reshape(2048, 256)))

    lane = lax.broadcasted_iota(jnp.int32, (128, 128), 1)

    def stat_send():
        table = jnp.zeros((128, 128), F32)
        for q in (0, 1):
            for b in (0, 1):
                v = lf[b, q * 128 : (q + 1) * 128, :]
                mean = jnp.mean(v, axis=1, keepdims=True)
                dev2 = jnp.sum(jnp.square(v - mean), axis=1, keepdims=True)
                table = jnp.where(lane == q * 8 + b * 2, mean, table)
                table = jnp.where(lane == q * 8 + b * 2 + 1, dev2, table)
        flipped = table.T
        sto[0] = flipped[0:8]
        sto[1] = flipped[8:16]
        routes = (
            (0, 1, 0, sib),
            (1, 0, 0, sib),
            (0, 0, 1, partner),
            (0, 1, 2, dev(xo, y, z8, 1 - c)),
            (1, 0, 2, dev(xt, y, z8, 1 - c)),
            (1, 1, 1, dev(xt, y, z8, c)),
        )
        for q, dest, slot, to in routes:
            j = dest * 3 + slot
            start(remote(sto.at[q], sti.at[dest, slot], st_send.at[j], st_recv.at[j], to))

    def stat_combine():
        for dest in (0, 1):
            for slot in (0, 1, 2):
                j = dest * 3 + slot
                remote(sto.at[0], sti.at[dest, slot], st_send.at[j], st_recv.at[j], sib).wait_recv()
        rows = []
        for q in (0, 1):
            for b in (0, 1):
                parts = [(sto, q, None, b), (sti, q, 0, b), (sti, q, 1, 1 - b), (sti, q, 2, 1 - b)]
                means, devs = [], []
                for ref, qq, slot, bb in parts:
                    block = ref[qq] if slot is None else ref[qq, slot]
                    means.append(block[bb * 2 : bb * 2 + 1])
                    devs.append(block[bb * 2 + 1 : bb * 2 + 2])
                centre = (means[0] + means[1] + means[2] + means[3]) * 0.25
                spread = devs[0] + devs[1] + devs[2] + devs[3]
                for m in means:
                    spread = spread + 512.0 * jnp.square(m - centre)
                rows.append(centre)
                rows.append(lax.rsqrt(spread * (1.0 / A) + layer_epsilon))
        for s in (0, 1):
            for g in (0, 1):
                rows.append(prm[s, 4 + g : 5 + g])
        rows.append(jnp.zeros((116, 128), F32))
        colm[...] = jnp.concatenate(rows, axis=0).T

    def mixer_mid(b):
        for q in (0, 1):
            k = (q * 2 + b) * 2
            centre, factor = colm[:, k : k + 1], colm[:, k + 1 : k + 2]
            tok = pl.ds(q * 128, 128)
            for s in (0, 1):
                for g in (0, 1):
                    n = s * 2 + g
                    cols = pl.ds(n * 128, 128)
                    v = (lf[b, tok, cols] - centre) * factor * prm[s, g : g + 1] + prm[s, 2 + g : 3 + g]
                    mixed = dot(msp[n], v.astype(BF16)) + colm[:, 8 + n : 9 + n]
                    hid2[b, tok, cols] = (gu[b, tok, cols] * mixed).astype(BF16)

    p2(GL, 0)
    p3(GL, 0)
    swap(GL).wait_recv()
    p1(GL, 1)
    ag_relay(0)
    p2(GL, 1)
    p3(GL, 1)
    p2(DN, 0)
    swap(DN).wait_recv()
    p1(DN, 1)
    p4(GL, 0)
    p3(DN, 0)
    p2(DN, 1)
    p4(GL, 1)
    p3(DN, 1)
    ag_wait_left(0)
    ag_wait_right(0)
    p5(GL, 0)

    @pl.loop(0, 2)
    def _(b):
        up_slot(0, b, 0)

    p2(UV, 0)
    swap(UV).wait_recv()
    p1(UV, 1)
    p4(DN, 0)
    p3(UV, 0)
    p5(GL, 1)

    @pl.loop(0, 2)
    def _(b):
        up_slot(0, b, 1)
        up_tail(0, b)

    p2(UV, 1)
    p4(DN, 1)
    p3(UV, 1)
    p2(MD, 0)
    swap(MD).wait_recv()
    p1(MD, 1)
    p5(DN, 0)
    p5(DN, 1)
    down(0, R, hid, wd_cols)
    p4(UV, 0)
    p3(MD, 0)
    down(0, L, hid, wd_cols)
    p2(MD, 1)
    rs_right(0)
    p3(MD, 1)
    swap_prm.wait_recv()
    swap_sp.wait_recv()
    causal = lax.broadcasted_iota(jnp.int32, (128, 128), 0) >= lane
    for s in (0, 1):
        for g in (0, 1):
            msp[s * 2 + g] = jnp.where(causal, sp2[s, g].astype(F32), 0.0).astype(BF16)
    rs_left(0, 0.5, m_gain)
    p4(UV, 1)
    ag_relay(1)
    p5(UV, 0)
    p5(UV, 1)
    ag_wait_left(1)
    mixer_up(L)
    p4(MD, 0)
    ag_wait_right(1)
    mixer_up(R)
    stat_send()
    p4(MD, 1)
    stat_combine()
    mixer_mid(R)
    p5(MD, 0)
    p5(MD, 1)
    down(1, R, hid2, wmd_cols)
    mixer_mid(L)
    down(1, L, hid2, wmd_cols)
    rs_right(1)
    rs_left(1, 1.0, gain_a)
    ag_wait_left(2)
    up(2, L)
    ag_relay(2)
    ag_wait_right(2)
    up(2, R)
    down(2, R, hid, wd_cols)
    down(2, L, hid, wd_cols)
    rs_right(2)
    rs_left(2, 0.5, None)

    for copy in sent:
        copy.wait_send()


def layer(stream, gain_b, gain_a, p_gate, p_lift, p_down, m_gain, m_u, m_v, l_gain, l_shift, spat, s_shift, m_down):
    vmem = pl.BlockSpec(memory_space=pltpu.VMEM)
    dma = pltpu.SemaphoreType.DMA
    return pl.pallas_call(
        kernel,
        out_shape=jax.ShapeDtypeStruct((128, 2048), BF16),
        in_specs=[vmem] * 14,
        out_specs=vmem,
        scratch_shapes=[
            pltpu.VMEM((2, 4, 4, 128, 896), BF16),
            pltpu.VMEM((2, 4, 4, 448, 128), BF16),
            pltpu.VMEM((2, 4, 4, 128, 512), BF16),
            pltpu.VMEM((2, 4, 4, 256, 128), BF16),
            pltpu.VMEM((4, 128, 128), BF16),
            pltpu.VMEM((2, 2, 128, 128), BF16),
            pltpu.VMEM((2, 8, 128), F32),
            pltpu.VMEM((3, 2, 2, 128, 2048), BF16),
            pltpu.VMEM((3, 2, 128, 2048), BF16),
            pltpu.VMEM((3, 2, 128, 2048), BF16),
            pltpu.VMEM((3, 128, 2048), BF16),
            pltpu.VMEM((3, 128, 2048), BF16),
            pltpu.VMEM((2, 128, 2048), F32),
            pltpu.VMEM((2, 256, 896), BF16),
            pltpu.VMEM((2, 256, 512), BF16),
            pltpu.VMEM((2, 256, 512), F32),
            pltpu.VMEM((2, 256, 512), F32),
            pltpu.VMEM((128, 2048), BF16),
            pltpu.VMEM((2, 8, 128), F32),
            pltpu.VMEM((2, 3, 8, 128), F32),
            pltpu.VMEM((128, 128), F32),
            dma((128,)), dma((128,)),
            dma((6,)), dma((6,)),
            dma((9 * CH,)), dma((9 * CH,)),
            dma((3 * (2 + CH),)), dma((3 * (2 + CH),)),
            dma((6,)), dma((6,)),
        ],
        compiler_params=pltpu.CompilerParams(
            collective_id=0, has_side_effects=True, vmem_limit_bytes=58 * 1024 * 1024
        ),
    )(
        stream, gain_b.reshape(1, -1), gain_a.reshape(1, -1), p_gate, p_lift, p_down, m_gain.reshape(1, -1),
        m_u, m_v, l_gain.reshape(2, 128), l_shift.reshape(2, 128), spat, s_shift, m_down,
    )


def solution(mesh):
    placed = (
        P(("rep", "fs", "tp"), None),
        P(),
        P(),
        P("fs", "tp"),
        P("fs", "tp"),
        P("tp", "fs"),
        P(),
        P("fs", "tp"),
        P("fs", "tp"),
        P("tp"),
        P("tp"),
        P("tp", None, None),
        P("tp", None),
        P("tp", "fs"),
    )
    return jax.shard_map(
        layer, mesh=mesh, in_specs=placed, out_specs=P(("rep", "fs", "tp"), None), check_vma=False
    )
```

time: 496 us -> 162 us (0.33)
  waiting for transfers between devices: 254 us -> 0 us
  Pallas kernels: 0 us -> 157 us
  blocking collectives: 157 us -> 0 us
  matrix products: 48 us -> 0 us
  between operations: 14 us -> 0.01 us
  other arithmetic: 12.1 us -> 0 us
    all_gather x7 -> x0, waiting for transfers between devices: 253 us -> none  [the longest x2 129 us: side_by_side(): lax.all_gather(both, axis, axis=dim, tiled=True)]
    pallas_call x0 -> x1, Pallas kernels: none -> 157 us  [layer(): pl.pallas_call(kernel, out_shape=jax.ShapeDtypeStruct((128, 2048), BF16),...]
    all_to_all x4 -> x0, blocking collectives: 135 us -> none  [the longest x2 83.9 us: sent_to_all(): return lax.all_to_all(copies, axis, split_axis=0, concat_axis=0, tiled=True)]
    dot_general x31 -> x0, matrix products: 48 us -> none  [the longest x24 25.3 us: rows_project(): jnp.dot(own_tokens[:, member * width:(member + 1) * width], weight_whole[...]
    psum x1 -> x0, blocking collectives: 22.8 us -> none  [token_mixer(): lax.psum((jnp.sum(lifted, axis=1), jnp.sum(lifted * lifted, axis=1)), 'tp')]
    reduce_sum x3 -> x0, other arithmetic: 9.37 us -> none  [norm_rows(): jnp.mean(widened * widened, axis=1, keepdims=True) + norm_epsilon]
  transfers between devices with their start and end apart: 8 -> 0, of which waited for: 5 -> 0; matrix products, arithmetic and copies ran while one was open for 6% -> 0% of each run, Pallas kernels for 0% -> 0%
where the time goes in v1:
time: 162 us
  Pallas kernels  157 us (97%)
  local copies, waits for them, and re-layouts  4.35 us (3%)
    pallas_call x1, Pallas kernels, layer(): pl.pallas_call(kernel, out_shape=jax.ShapeDtypeStruct((128, 2048), BF16),...  157 us
    unnamed x5, local copies, waits for them, and re-layouts  4.35 us

profile of v1, /device:TPU:1, one launch (start us, length us, event | category | flops | bytes accessed | tf_op | source)
XLA Modules:
  0.0 161.7 jit_solution(14346386974176164007)
XLA Ops:
  0.0 0.0 copy-start
  0.0 1.7 %copy.15.p_gate = bf16[128,448]{1,0:T(8,128)(2,1)} copy(bf16[128,448]{0,1:T(8,128)(2,1)} %param.17) | data formatting | bytes 229376 | tf_op args[3]
  1.7 0.0 copy-done
  1.7 0.8 copy.16.p_lift
  2.5 157.4 %shard_map.136 = bf16[128,2048]{1,0:T(8,128)(2,1)} custom-call(bf16[128,2048]{1,0:T(8,128)(2,1)} %stream.1, f32[1,2048]{1,0:T(1,128)} %bitcast.5, f32[1,2048]{1,0:T(1,128)} %bitcast.6, bf16[128,448]{1,0:T(8,128)(2,1)} %copy.15.p_gate, bf16[128,448]{1,0:T(8,128)(2,1)} %copy.16.p_lift, bf16[448,128]{1,0:T(8,128)(2,1)} %p_down.1, f32[1,2048]{1,0:T(1,128)} %bitcast.7, ...), custom_call_target="tpu_custom_call" | custom-call | tf_op jit(solution)/shard_map/pallas_call | solution.py:486
  159.9 1.9 %copy.18 = bf16[128,2048]{1,0:T(8,128)(2,1)} copy(bf16[128,2048]{1,0:T(8,128)(2,1)} %shard_map.136) | data formatting | bytes 1048576
Async XLA Ops:
  0.0 1.7 %copy-start = (bf16[128,448]{0,1:T(8,128)(2,1)S(1)}, bf16[128,448]{0,1:T(8,128)(2,1)}, u32[]{:S(2)}) copy-start(bf16[128,448]{0,1:T(8,128)(2,1)} %param.18) | copy-start | bytes 344068

commit v2 on v1

--- a/solution.py
+++ b/solution.py
@@ -40,7 +40,7 @@
     out,
     wgl, wd, wuv, wmd, msp, sp2, prm,
     xs, po, ps, pc, pr, acc, hid, hid2, gu, lf, res, sto, sti, colm,
-    w_send, w_recv, sw_send, sw_recv, ag_send, ag_recv, rs_send, rs_recv, st_send, st_recv,
+    out_sem, w_send, w_recv, sw_send, sw_recv, ag_send, ag_recv, rs_send, rs_recv, st_send, st_recv,
 ):
     rep, fs, tp = lax.axis_index("rep"), lax.axis_index("fs"), lax.axis_index("tp")
     x, c = tp // 2, tp % 2
@@ -170,14 +170,13 @@
         j = r * 3 * CH + 2 * CH + ch
         return remote(xs.at[r, R, 1, rows], xs.at[r, R, 1, rows], ag_send.at[j], ag_recv.at[j], sib)
 
-    def rs_d2d(r, b):
-        j = r * (2 + CH) + b
-        return remote(po.at[r, b], ps.at[r, b], rs_send.at[j], rs_recv.at[j], sib)
-
-    def rs_ici(r, ch):
-        rows = pl.ds(ch * CROWS, CROWS)
-        j = r * (2 + CH) + 2 + ch
-        return remote(pc.at[r, rows], pr.at[r, rows], rs_send.at[j], rs_recv.at[j], partner)
+    def rs_d2d(r, b, half):
+        j = r * 6 + b * 2 + half
+        return remote(po.at[r, b, half], ps.at[r, b, half], rs_send.at[j], rs_recv.at[j], sib)
+
+    def rs_ici(r, half):
+        j = r * 6 + 4 + half
+        return remote(pc.at[r, half], pr.at[r, half], rs_send.at[j], rs_recv.at[j], partner)
 
     def normed(rows, gain):
         factor = lax.rsqrt(jnp.mean(rows * rows, axis=1, keepdims=True) + norm_epsilon)
@@ -204,11 +203,11 @@
         [
             piece
             for j in range(3)
-            for piece in (p_gate[:, j * 128 : (j + 1) * 128], p_lift[:, j * 128 : (j + 1) * 128])
+            for piece in (p_gate[j * 128 : (j + 1) * 128], p_lift[j * 128 : (j + 1) * 128])
         ]
-        + [p_gate[:, 384:448], p_lift[:, 384:448]],
-        axis=1,
-    )
+        + [p_gate[384:448], p_lift[384:448]],
+        axis=0,
+    ).T
 
     @pl.loop(0, 128 // STEP)
     def _(i):
@@ -225,18 +224,15 @@
 
     pl.semaphore_wait(barrier, len(greeted))
 
+    swap_prm = remote(prm.at[0], prm.at[1], sw_send.at[4], sw_recv.at[4], swap_to)
+    swap_sp = remote(sp2.at[0], sp2.at[1], sw_send.at[5], sw_recv.at[5], swap_to)
     p1(GL, 0)
     start(swap(GL))
+    start(swap(DN))
     for ch in range(CH):
         ag_send_chunk(0, ch)
-    p1(DN, 0)
-    start(swap(DN))
-    p1(UV, 0)
     start(swap(UV))
-    p1(MD, 0)
     start(swap(MD))
-    swap_prm = remote(prm.at[0], prm.at[1], sw_send.at[4], sw_recv.at[4], swap_to)
-    swap_sp = remote(sp2.at[0], sp2.at[1], sw_send.at[5], sw_recv.at[5], swap_to)
     start(swap_prm)
     start(swap_sp)
 
@@ -275,47 +271,63 @@
     def wmd_cols(zz, yy):
         return jnp.concatenate([wmd[0, zz, yy], wmd[1, zz, yy]], axis=0)
 
-    def down(r, b, lhs, columns_of):
-        @pl.loop(0, 8)
+    def down(r, b, half, lhs, columns_of):
+        @pl.loop(0, 4, unroll=2)
         def _(n):
-            zz, yy = n // 2, (n % 2) * 2
+            zz, yy = half * 2 + n // 2, (n % 2) * 2
             rhs = jnp.concatenate([columns_of(zz, yy), columns_of(zz, yy + 1)], axis=1)
             o = dot(lhs[b], rhs)
             cols = pl.ds(pl.multiple_of(n * 256, 256), 256)
-            acc[b, :, cols] = o[:128]
-            po[r, b, :, cols] = o[128:].astype(BF16)
-
-        start(rs_d2d(r, b))
-
-    def rs_right(r):
-        rs_d2d(r, R).wait_recv()
+            acc[b, half, :, cols] = o[:128]
+            po[r, b, half, :, cols] = o[128:].astype(BF16)
+
+        start(rs_d2d(r, b, half))
+
+    def rs_right(r, half):
+        rs_d2d(r, R, half).wait_recv()
+
+        @pl.loop(0, 128 // STEP)
+        def _(i):
+            rows = pl.ds(i * STEP, STEP)
+            pc[r, half, rows, :] = (acc[R, half, rows, :] + ps[r, R, half, rows, :].astype(F32)).astype(BF16)
+
+        start(rs_ici(r, half))
+
+    def down_all(r, lhs, columns_of):
+        down(r, R, 0, lhs, columns_of)
+        down(r, R, 1, lhs, columns_of)
+        rs_right(r, 0)
+        down(r, L, 0, lhs, columns_of)
+        rs_right(r, 1)
+        down(r, L, 1, lhs, columns_of)
+
+    def rs_left(r, coefficient, gain):
+        for half in (0, 1):
+            rs_d2d(r, L, half).wait_recv()
+        for half in (0, 1):
+            rs_ici(r, half).wait_recv()
         for ch in range(CH):
 
             @pl.loop(0, CROWS // STEP)
             def _(i):
                 rows = pl.ds(ch * CROWS + i * STEP, STEP)
-                pc[r, rows, :] = (acc[R, rows, :] + ps[r, R, rows, :].astype(F32)).astype(BF16)
-
-            start(rs_ici(r, ch))
-
-    def rs_left(r, coefficient, gain):
-        rs_d2d(r, L).wait_recv()
-        for ch in range(CH):
-            rs_ici(r, ch).wait_recv()
-
-            @pl.loop(0, CROWS // STEP)
-            def _(i):
-                rows = pl.ds(ch * CROWS + i * STEP, STEP)
-                delta = acc[L, rows, :] + ps[r, L, rows, :].astype(F32) + pr[r, rows, :].astype(F32)
+                delta = jnp.concatenate(
+                    [
+                        acc[L, half, rows, :] + ps[r, L, half, rows, :].astype(F32) + pr[r, half, rows, :].astype(F32)
+                        for half in (0, 1)
+                    ],
+                    axis=1,
+                )
                 new = (res[rows, :].astype(F32) + coefficient * delta).astype(BF16)
-                if gain is None:
-                    out[rows, :] = new
-                else:
-                    res[rows, :] = new
+                res[rows, :] = new
+                if gain is not None:
                     xs[r + 1, L, 0, rows, :] = normed(new.astype(F32), gain)
 
+            rows = pl.ds(ch * CROWS, CROWS)
             if gain is not None:
                 ag_send_chunk(r + 1, ch)
+            else:
+                pltpu.make_async_copy(res.at[rows], out.at[rows], out_sem.at[ch]).start()
 
     def mixer_up(b):
         @pl.loop(0, 2)
@@ -390,18 +402,23 @@
                     hid2[b, tok, cols] = (gu[b, tok, cols] * mixed).astype(BF16)
 
     p2(GL, 0)
-    p3(GL, 0)
+    p1(DN, 0)
     swap(GL).wait_recv()
     p1(GL, 1)
-    ag_relay(0)
+    p3(GL, 0)
+    p2(DN, 0)
     p2(GL, 1)
-    p3(GL, 1)
-    p2(DN, 0)
     swap(DN).wait_recv()
     p1(DN, 1)
+    p1(UV, 0)
     p4(GL, 0)
+    p3(GL, 1)
+    p2(DN, 1)
+    p2(UV, 0)
+    swap(UV).wait_recv()
+    p1(UV, 1)
     p3(DN, 0)
-    p2(DN, 1)
+    ag_relay(0)
     p4(GL, 1)
     p3(DN, 1)
     ag_wait_left(0)
@@ -412,11 +429,9 @@
     def _(b):
         up_slot(0, b, 0)
 
-    p2(UV, 0)
-    swap(UV).wait_recv()
-    p1(UV, 1)
     p4(DN, 0)
-    p3(UV, 0)
+    p2(UV, 1)
+    p1(MD, 0)
     p5(GL, 1)
 
     @pl.loop(0, 2)
@@ -424,29 +439,27 @@
         up_slot(0, b, 1)
         up_tail(0, b)
 
-    p2(UV, 1)
     p4(DN, 1)
-    p3(UV, 1)
+    p3(UV, 0)
     p2(MD, 0)
     swap(MD).wait_recv()
     p1(MD, 1)
-    p5(DN, 0)
-    p5(DN, 1)
-    down(0, R, hid, wd_cols)
-    p4(UV, 0)
-    p3(MD, 0)
-    down(0, L, hid, wd_cols)
-    p2(MD, 1)
-    rs_right(0)
-    p3(MD, 1)
+    p3(UV, 1)
     swap_prm.wait_recv()
     swap_sp.wait_recv()
     causal = lax.broadcasted_iota(jnp.int32, (128, 128), 0) >= lane
     for s in (0, 1):
         for g in (0, 1):
             msp[s * 2 + g] = jnp.where(causal, sp2[s, g].astype(F32), 0.0).astype(BF16)
+    p5(DN, 0)
+    p5(DN, 1)
+    down_all(0, hid, wd_cols)
+    p4(UV, 0)
+    p3(MD, 0)
+    p2(MD, 1)
     rs_left(0, 0.5, m_gain)
     p4(UV, 1)
+    p3(MD, 1)
     ag_relay(1)
     p5(UV, 0)
     p5(UV, 1)
@@ -459,23 +472,22 @@
     p4(MD, 1)
     stat_combine()
     mixer_mid(R)
+    mixer_mid(L)
     p5(MD, 0)
     p5(MD, 1)
-    down(1, R, hid2, wmd_cols)
-    mixer_mid(L)
-    down(1, L, hid2, wmd_cols)
-    rs_right(1)
+    down_all(1, hid2, wmd_cols)
     rs_left(1, 1.0, gain_a)
     ag_wait_left(2)
     up(2, L)
     ag_relay(2)
     ag_wait_right(2)
     up(2, R)
-    down(2, R, hid, wd_cols)
-    down(2, L, hid, wd_cols)
-    rs_right(2)
+    down_all(2, hid, wd_cols)
     rs_left(2, 0.5, None)
 
+    for ch in range(CH):
+        rows = pl.ds(ch * CROWS, CROWS)
+        pltpu.make_async_copy(res.at[rows], out.at[rows], out_sem.at[ch]).wait()
     for copy in sent:
         copy.wait_send()
 
@@ -487,7 +499,7 @@
         kernel,
         out_shape=jax.ShapeDtypeStruct((128, 2048), BF16),
         in_specs=[vmem] * 14,
-        out_specs=vmem,
+        out_specs=pl.BlockSpec(memory_space=pl.ANY),
         scratch_shapes=[
             pltpu.VMEM((2, 4, 4, 128, 896), BF16),
             pltpu.VMEM((2, 4, 4, 448, 128), BF16),
@@ -497,11 +509,11 @@
             pltpu.VMEM((2, 2, 128, 128), BF16),
             pltpu.VMEM((2, 8, 128), F32),
             pltpu.VMEM((3, 2, 2, 128, 2048), BF16),
-            pltpu.VMEM((3, 2, 128, 2048), BF16),
-            pltpu.VMEM((3, 2, 128, 2048), BF16),
-            pltpu.VMEM((3, 128, 2048), BF16),
-            pltpu.VMEM((3, 128, 2048), BF16),
-            pltpu.VMEM((2, 128, 2048), F32),
+            pltpu.VMEM((3, 2, 2, 128, 1024), BF16),
+            pltpu.VMEM((3, 2, 2, 128, 1024), BF16),
+            pltpu.VMEM((3, 2, 128, 1024), BF16),
+            pltpu.VMEM((3, 2, 128, 1024), BF16),
+            pltpu.VMEM((2, 2, 128, 1024), F32),
             pltpu.VMEM((2, 256, 896), BF16),
             pltpu.VMEM((2, 256, 512), BF16),
             pltpu.VMEM((2, 256, 512), F32),
@@ -510,17 +522,18 @@
             pltpu.VMEM((2, 8, 128), F32),
             pltpu.VMEM((2, 3, 8, 128), F32),
             pltpu.VMEM((128, 128), F32),
+            dma((CH,)),
             dma((128,)), dma((128,)),
             dma((6,)), dma((6,)),
             dma((9 * CH,)), dma((9 * CH,)),
-            dma((3 * (2 + CH),)), dma((3 * (2 + CH),)),
+            dma((18,)), dma((18,)),
             dma((6,)), dma((6,)),
         ],
         compiler_params=pltpu.CompilerParams(
             collective_id=0, has_side_effects=True, vmem_limit_bytes=58 * 1024 * 1024
         ),
     )(
-        stream, gain_b.reshape(1, -1), gain_a.reshape(1, -1), p_gate, p_lift, p_down, m_gain.reshape(1, -1),
+        stream, gain_b.reshape(1, -1), gain_a.reshape(1, -1), p_gate.T, p_lift.T, p_down, m_gain.reshape(1, -1),
         m_u, m_v, l_gain.reshape(2, 128), l_shift.reshape(2, 128), spat, s_shift, m_down,
     )
 

time: 162 us -> 145 us (0.90)
  Pallas kernels: 157 us -> 143 us
  local copies, waits for them, and re-layouts: 4.35 us -> 1.88 us
    pallas_call x1, Pallas kernels: 157 us -> 143 us  [layer(): pl.pallas_call(kernel, out_shape=jax.ShapeDtypeStruct((128, 2048), BF16),...]
    unnamed x5 -> x1, local copies, waits for them, and re-layouts: 4.35 us -> 1.88 us
where the time goes in v2:
time: 145 us
  Pallas kernels  143 us (99%)
  local copies, waits for them, and re-layouts  1.88 us (1%)
    pallas_call x1, Pallas kernels, layer(): pl.pallas_call(kernel, out_shape=jax.ShapeDtypeStruct((128, 2048), BF16),...  143 us

profile of v2, /device:TPU:1, one launch (start us, length us, event | category | flops | bytes accessed | tf_op | source)
XLA Modules:
  0.0 145.3 jit_solution(6578197992880491203)
XLA Ops:
  0.0 143.4 %shard_map.136 = bf16[128,2048]{1,0:T(8,128)(2,1)} custom-call(bf16[128,2048]{1,0:T(8,128)(2,1)} %stream.1, f32[1,2048]{1,0:T(1,128)} %bitcast.9, f32[1,2048]{1,0:T(1,128)} %bitcast.10, bf16[448,128]{1,0:T(8,128)(2,1)} %bitcast.7, bf16[448,128]{1,0:T(8,128)(2,1)} %bitcast.8, bf16[448,128]{1,0:T(8,128)(2,1)} %p_down.1, f32[1,2048]{1,0:T(1,128)} %bitcast.11, ...), custom_call_target="tpu_custom_call" | custom-call | tf_op jit(solution)/shard_map/pallas_call | solution.py:498
  143.4 1.9 %copy.16 = bf16[128,2048]{1,0:T(8,128)(2,1)} copy(bf16[128,2048]{1,0:T(8,128)(2,1)} %shard_map.136) | data formatting | bytes 1048576

commit v3 on v2

--- a/solution.py
+++ b/solution.py
@@ -31,16 +31,16 @@
     return jnp.dot(a, b, preferred_element_type=F32)
 
 
-def widx(w, s, part, phase, i):
-    return (((w * 2 + s) * 2 + part) * 2 + phase) * 4 + i
+def recv_index(w, s, part, phase, i):
+    return ((w * 3 + s * 2 + phase - s) * 2 + part) * 3 + min(i, 2)
 
 
 def kernel(
     stream, gain_b, gain_a, p_gate, p_lift, p_down, m_gain, m_u, m_v, l_gain, l_shift, spat, s_shift, m_down,
     out,
-    wgl, wd, wuv, wmd, msp, sp2, prm,
+    wgl, wd, wuv, wmd, rgl, rd, ruv, rmd, msp, sp2, prm,
     xs, po, ps, pc, pr, acc, hid, hid2, gu, lf, res, sto, sti, colm,
-    out_sem, w_send, w_recv, sw_send, sw_recv, ag_send, ag_recv, rs_send, rs_recv, st_send, st_recv,
+    w_send, w_recv, x_recv, sw_send, sw_recv, ag_send, ag_recv, rs_send, rs_recv, st_send, st_recv,
 ):
     rep, fs, tp = lax.axis_index("rep"), lax.axis_index("fs"), lax.axis_index("tp")
     x, c = tp // 2, tp % 2
@@ -58,6 +58,8 @@
     z_plus, z_minus = dev(x, y, (z8 + 1) % 8, c), dev(x, y, (z8 + 7) % 8, c)
     swap_to = dev((x + 2) % 4, y, z8, c)
     weights = (wgl, wd, wuv, wmd)
+    relays = (rgl, rd, ruv, rmd)
+    x_dirs = (dev((x + 1) % 4, y, z8, c), dev((x + 3) % 4, y, z8, c))
 
     barrier = pltpu.get_barrier_semaphore()
     greeted = (
@@ -67,8 +69,6 @@
     for other in greeted:
         pl.semaphore_signal(barrier, inc=1, device_id=other, device_id_type=MESH)
 
-    sent = []
-
     def remote(src, dst, ssem, rsem, to):
         return pltpu.make_async_remote_copy(
             src_ref=src, dst_ref=dst, send_sem=ssem, recv_sem=rsem, device_id=to, device_id_type=MESH
@@ -76,7 +76,6 @@
 
     def start(copy):
         copy.start()
-        sent.append(copy)
 
     def region(w, s, part, phase, pos, sub):
         n = W_ROWS[w] // 2
@@ -99,20 +98,20 @@
         me, plus, minus = ring(part, phase)
         pos = (me, me, (me + 3) % 4, (me + 1) % 4)[i]
         block = region(w, s, part, phase, pos, (None, None, 0, 1)[i])
-        j = widx(w, s, part, phase, i)
-        start(remote(block, block, w_send.at[j], w_recv.at[j], (plus, minus, plus, minus)[i]))
+        j = recv_index(w, s, part, phase, i)
+        start(remote(block, block, w_send.at[w * 4 + s + phase], w_recv.at[j], (plus, minus, plus, minus)[i]))
 
     def w_wait(w, s, part, phase, i):
         me, plus, minus = ring(part, phase)
-        pos = ((me + 3) % 4, (me + 1) % 4, (me + 2) % 4, (me + 2) % 4)[i]
-        block = region(w, s, part, phase, pos, (None, None, 0, 1)[i])
-        j = widx(w, s, part, phase, i)
-        remote(block, block, w_send.at[j], w_recv.at[j], plus).wait_recv()
-
-    def p1(w, s):
+        pos = ((me + 3) % 4, (me + 1) % 4, (me + 2) % 4)[i]
+        block = region(w, s, part, phase, pos, None)
+        j = recv_index(w, s, part, phase, i)
+        remote(block, block, w_send.at[w * 4 + s + phase], w_recv.at[j], plus).wait_recv()
+
+    def p1(w):
         for part in (0, 1):
             for i in (0, 1):
-                w_start(w, s, part, 0, i)
+                w_start(w, 0, part, 0, i)
 
     def forward(w, s, phase):
         for part in (0, 1):
@@ -120,13 +119,32 @@
                 w_wait(w, s, part, phase, i)
                 w_start(w, s, part, phase, i + 2)
 
-    def p2(w, s):
-        forward(w, s, 0)
+    def p2(w):
+        forward(w, 0, 0)
+
+    def x_copy(w, part, relayed):
+        me = ring(part, 1)[0]
+        block = region(w, 0, part, 1, me, None)
+        if relayed:
+            src, dst = relays[w].at[part], region(w, 1, part, 1, me, None)
+        else:
+            src, dst = block, relays[w].at[part]
+        return remote(src, dst, w_send.at[w * 4 + 3], x_recv.at[w * 4 + relayed * 2 + part], x_dirs[part])
+
+    def px(w):
+        for part in (0, 1):
+            w_wait(w, 0, part, 0, 2)
+            start(x_copy(w, part, 0))
+
+    def xr(w):
+        for part in (0, 1):
+            x_copy(w, part, 0).wait_recv()
+            start(x_copy(w, part, 1))
 
     def p3(w, s):
         for part in (0, 1):
-            w_wait(w, s, part, 0, 2)
-            w_wait(w, s, part, 0, 3)
+            if s == 1:
+                x_copy(w, part, 1).wait_recv()
             for i in (0, 1):
                 w_start(w, s, part, 1, i)
 
@@ -136,68 +154,68 @@
     def p5(w, s):
         for part in (0, 1):
             w_wait(w, s, part, 1, 2)
-            w_wait(w, s, part, 1, 3)
-
-    def swap(w):
-        ref = weights[w]
-        return remote(ref.at[0, zl, y], ref.at[1, zl, y], sw_send.at[w], sw_recv.at[w], swap_to)
-
-    def ag_own(r, ch):
+
+    def wait_sent():
+        def drained(ref, sem):
+            remote(ref, ref, sem, x_recv.at[0], sib).wait_send()
+
+        for w in range(4):
+            ref = weights[w]
+            drained(ref.at[0, 0, 0:3], w_send.at[w * 4])
+            drained(ref.at[0, 0:3], w_send.at[w * 4 + 1])
+            drained(ref.at[1, 0:3], w_send.at[w * 4 + 2])
+            drained(ref.at[0, 0:2], w_send.at[w * 4 + 3])
+        for r in range(3):
+            drained(xs.at[r, 0], ag_send.at[r * 2])
+            drained(xs.at[r, 0, 0], ag_send.at[r * 2 + 1])
+            drained(po.at[r], rs_send.at[r * 2])
+            drained(pc.at[r], rs_send.at[r * 2 + 1])
+        drained(sti, st_send.at[0])
+        swap_prm.wait_send()
+        swap_sp.wait_send()
+
+    def ag_ici(r, ch):
         rows = pl.ds(ch * CROWS, CROWS)
-        j = r * 3 * CH + ch
-        return (
-            remote(xs.at[r, L, 0, rows], xs.at[r, R, 0, rows], ag_send.at[j], ag_recv.at[j], partner),
-            remote(xs.at[r, L, 0, rows], xs.at[r, L, 1, rows], ag_send.at[j + CH], ag_recv.at[j + CH], sib),
-        )
-
-    def ag_fwd(r, ch):
-        rows = pl.ds(ch * CROWS, CROWS)
-        j = r * 3 * CH + 2 * CH + ch
-        return remote(xs.at[r, R, 0, rows], xs.at[r, R, 1, rows], ag_send.at[j], ag_recv.at[j], sib)
-
-    def ag_recv_partner(r, ch):
-        rows = pl.ds(ch * CROWS, CROWS)
-        j = r * 3 * CH + ch
-        return remote(xs.at[r, R, 0, rows], xs.at[r, R, 0, rows], ag_send.at[j], ag_recv.at[j], partner)
-
-    def ag_recv_sib(r, ch):
-        rows = pl.ds(ch * CROWS, CROWS)
-        j = r * 3 * CH + CH + ch
-        return remote(xs.at[r, L, 1, rows], xs.at[r, L, 1, rows], ag_send.at[j], ag_recv.at[j], sib)
-
-    def ag_recv_fwd(r, ch):
-        rows = pl.ds(ch * CROWS, CROWS)
-        j = r * 3 * CH + 2 * CH + ch
-        return remote(xs.at[r, R, 1, rows], xs.at[r, R, 1, rows], ag_send.at[j], ag_recv.at[j], sib)
+        return remote(
+            xs.at[r, L, 0, rows], xs.at[r, R, 0, rows], ag_send.at[r * 2], ag_recv.at[r * (CH + 2) + ch], partner
+        )
+
+    def ag_d2d(r, rows):
+        return remote(
+            xs.at[r, L, 0, rows], xs.at[r, L, 1, rows], ag_send.at[r * 2], ag_recv.at[r * (CH + 2) + CH], sib
+        )
+
+    def ag_fwd(r, rows):
+        return remote(
+            xs.at[r, R, 0, rows], xs.at[r, R, 1, rows], ag_send.at[r * 2 + 1], ag_recv.at[r * (CH + 2) + CH + 1], sib
+        )
 
     def rs_d2d(r, b, half):
-        j = r * 6 + b * 2 + half
-        return remote(po.at[r, b, half], ps.at[r, b, half], rs_send.at[j], rs_recv.at[j], sib)
+        return remote(
+            po.at[r, b, half], ps.at[r, b, half], rs_send.at[r * 2], rs_recv.at[r * 4 + (half if b == R else 2)], sib
+        )
 
     def rs_ici(r, half):
-        j = r * 6 + 4 + half
-        return remote(pc.at[r, half], pr.at[r, half], rs_send.at[j], rs_recv.at[j], partner)
+        return remote(pc.at[r, half], pr.at[r, half], rs_send.at[r * 2 + 1], rs_recv.at[r * 4 + 3], partner)
 
     def normed(rows, gain):
         factor = lax.rsqrt(jnp.mean(rows * rows, axis=1, keepdims=True) + norm_epsilon)
         return (rows * factor * gain[...]).astype(BF16)
 
     def ag_send_chunk(r, ch):
-        for copy in ag_own(r, ch):
-            start(copy)
+        start(ag_ici(r, ch))
+        start(ag_d2d(r, pl.ds(ch * CROWS, CROWS)))
 
     def ag_wait_left(r):
-        for ch in range(CH):
-            ag_recv_sib(r, ch).wait_recv()
+        ag_d2d(r, pl.ds(0, 128)).wait_recv()
 
     def ag_relay(r):
         for ch in range(CH):
-            ag_recv_partner(r, ch).wait_recv()
-            start(ag_fwd(r, ch))
+            ag_ici(r, ch).wait_recv()
+            start(ag_fwd(r, pl.ds(ch * CROWS, CROWS)))
 
     def ag_wait_right(r):
-        for ch in range(CH):
-            ag_recv_fwd(r, ch).wait_recv()
+        ag_fwd(r, pl.ds(0, 128)).wait_recv()
 
     wgl[0, zl, y] = jnp.concatenate(
         [
@@ -224,17 +242,13 @@
 
     pl.semaphore_wait(barrier, len(greeted))
 
-    swap_prm = remote(prm.at[0], prm.at[1], sw_send.at[4], sw_recv.at[4], swap_to)
-    swap_sp = remote(sp2.at[0], sp2.at[1], sw_send.at[5], sw_recv.at[5], swap_to)
-    p1(GL, 0)
-    start(swap(GL))
-    start(swap(DN))
+    swap_prm = remote(prm.at[0], prm.at[1], sw_send.at[0], sw_recv.at[0], swap_to)
+    swap_sp = remote(sp2.at[0], sp2.at[1], sw_send.at[1], sw_recv.at[1], swap_to)
+    p1(GL)
+    start(swap_prm)
+    start(swap_sp)
     for ch in range(CH):
         ag_send_chunk(0, ch)
-    start(swap(UV))
-    start(swap(MD))
-    start(swap_prm)
-    start(swap_sp)
 
     def batch_x(r, b):
         return xs[r, b].reshape(256, 2048)
@@ -302,10 +316,8 @@
         down(r, L, 1, lhs, columns_of)
 
     def rs_left(r, coefficient, gain):
-        for half in (0, 1):
-            rs_d2d(r, L, half).wait_recv()
-        for half in (0, 1):
-            rs_ici(r, half).wait_recv()
+        remote(po.at[r, L], ps.at[r, L], rs_send.at[r * 2], rs_recv.at[r * 4 + 2], sib).wait_recv()
+        remote(pc.at[r], pr.at[r], rs_send.at[r * 2 + 1], rs_recv.at[r * 4 + 3], partner).wait_recv()
         for ch in range(CH):
 
             @pl.loop(0, CROWS // STEP)
@@ -319,15 +331,15 @@
                     axis=1,
                 )
                 new = (res[rows, :].astype(F32) + coefficient * delta).astype(BF16)
-                res[rows, :] = new
-                if gain is not None:
+                if gain is None:
+                    out[rows, :] = new
+                else:
+                    res[rows, :] = new
                     xs[r + 1, L, 0, rows, :] = normed(new.astype(F32), gain)
 
             rows = pl.ds(ch * CROWS, CROWS)
             if gain is not None:
                 ag_send_chunk(r + 1, ch)
-            else:
-                pltpu.make_async_copy(res.at[rows], out.at[rows], out_sem.at[ch]).start()
 
     def mixer_up(b):
         @pl.loop(0, 2)
@@ -359,14 +371,10 @@
             (1, 1, 1, dev(xt, y, z8, c)),
         )
         for q, dest, slot, to in routes:
-            j = dest * 3 + slot
-            start(remote(sto.at[q], sti.at[dest, slot], st_send.at[j], st_recv.at[j], to))
+            start(remote(sto.at[q], sti.at[dest, slot], st_send.at[0], st_recv.at[0], to))
 
     def stat_combine():
-        for dest in (0, 1):
-            for slot in (0, 1, 2):
-                j = dest * 3 + slot
-                remote(sto.at[0], sti.at[dest, slot], st_send.at[j], st_recv.at[j], sib).wait_recv()
+        remote(sti, sti, st_send.at[0], st_recv.at[0], sib).wait_recv()
         rows = []
         for q in (0, 1):
             for b in (0, 1):
@@ -401,26 +409,19 @@
                     mixed = dot(msp[n], v.astype(BF16)) + colm[:, 8 + n : 9 + n]
                     hid2[b, tok, cols] = (gu[b, tok, cols] * mixed).astype(BF16)
 
-    p2(GL, 0)
-    p1(DN, 0)
-    swap(GL).wait_recv()
-    p1(GL, 1)
+    p2(GL)
+    p1(DN)
+    px(GL)
     p3(GL, 0)
-    p2(DN, 0)
-    p2(GL, 1)
-    swap(DN).wait_recv()
-    p1(DN, 1)
-    p1(UV, 0)
+    p2(DN)
+    p1(UV)
     p4(GL, 0)
-    p3(GL, 1)
-    p2(DN, 1)
-    p2(UV, 0)
-    swap(UV).wait_recv()
-    p1(UV, 1)
+    xr(GL)
+    px(DN)
     p3(DN, 0)
+    p2(UV)
+    p1(MD)
     ag_relay(0)
-    p4(GL, 1)
-    p3(DN, 1)
     ag_wait_left(0)
     ag_wait_right(0)
     p5(GL, 0)
@@ -430,8 +431,14 @@
         up_slot(0, b, 0)
 
     p4(DN, 0)
-    p2(UV, 1)
-    p1(MD, 0)
+    p3(GL, 1)
+    xr(DN)
+    px(UV)
+    p2(MD)
+    p4(GL, 1)
+    p3(DN, 1)
+    px(MD)
+    xr(UV)
     p5(GL, 1)
 
     @pl.loop(0, 2)
@@ -441,9 +448,7 @@
 
     p4(DN, 1)
     p3(UV, 0)
-    p2(MD, 0)
-    swap(MD).wait_recv()
-    p1(MD, 1)
+    xr(MD)
     p3(UV, 1)
     swap_prm.wait_recv()
     swap_sp.wait_recv()
@@ -456,7 +461,6 @@
     down_all(0, hid, wd_cols)
     p4(UV, 0)
     p3(MD, 0)
-    p2(MD, 1)
     rs_left(0, 0.5, m_gain)
     p4(UV, 1)
     p3(MD, 1)
@@ -485,11 +489,7 @@
     down_all(2, hid, wd_cols)
     rs_left(2, 0.5, None)
 
-    for ch in range(CH):
-        rows = pl.ds(ch * CROWS, CROWS)
-        pltpu.make_async_copy(res.at[rows], out.at[rows], out_sem.at[ch]).wait()
-    for copy in sent:
-        copy.wait_send()
+    wait_sent()
 
 
 def layer(stream, gain_b, gain_a, p_gate, p_lift, p_down, m_gain, m_u, m_v, l_gain, l_shift, spat, s_shift, m_down):
@@ -497,14 +497,18 @@
     dma = pltpu.SemaphoreType.DMA
     return pl.pallas_call(
         kernel,
-        out_shape=jax.ShapeDtypeStruct((128, 2048), BF16),
+        out_shape=pltpu.VMEM((128, 2048), BF16),
         in_specs=[vmem] * 14,
-        out_specs=pl.BlockSpec(memory_space=pl.ANY),
+        out_specs=vmem,
         scratch_shapes=[
             pltpu.VMEM((2, 4, 4, 128, 896), BF16),
             pltpu.VMEM((2, 4, 4, 448, 128), BF16),
             pltpu.VMEM((2, 4, 4, 128, 512), BF16),
             pltpu.VMEM((2, 4, 4, 256, 128), BF16),
+            pltpu.VMEM((2, 4, 64, 896), BF16),
+            pltpu.VMEM((2, 4, 224, 128), BF16),
+            pltpu.VMEM((2, 4, 64, 512), BF16),
+            pltpu.VMEM((2, 4, 128, 128), BF16),
             pltpu.VMEM((4, 128, 128), BF16),
             pltpu.VMEM((2, 2, 128, 128), BF16),
             pltpu.VMEM((2, 8, 128), F32),
@@ -522,12 +526,11 @@
             pltpu.VMEM((2, 8, 128), F32),
             pltpu.VMEM((2, 3, 8, 128), F32),
             pltpu.VMEM((128, 128), F32),
-            dma((CH,)),
-            dma((128,)), dma((128,)),
-            dma((6,)), dma((6,)),
-            dma((9 * CH,)), dma((9 * CH,)),
-            dma((18,)), dma((18,)),
-            dma((6,)), dma((6,)),
+            dma((16,)), dma((72,)), dma((16,)),
+            dma((2,)), dma((2,)),
+            dma((6,)), dma((3 * (CH + 2),)),
+            dma((6,)), dma((12,)),
+            dma((1,)), dma((1,)),
         ],
         compiler_params=pltpu.CompilerParams(
             collective_id=0, has_side_effects=True, vmem_limit_bytes=58 * 1024 * 1024

time: 145 us -> 135 us (0.931)
  Pallas kernels: 143 us -> 134 us
    pallas_call x1, Pallas kernels: 143 us -> 134 us  [layer(): pl.pallas_call(kernel, out_shape=pltpu.VMEM((128, 2048), BF16), in_specs=...]
where the time goes in v3:
time: 135 us
  Pallas kernels  134 us (99%)
    pallas_call x1, Pallas kernels, layer(): pl.pallas_call(kernel, out_shape=pltpu.VMEM((128, 2048), BF16), in_specs=...  134 us

profile of v3, /device:TPU:1, one launch (start us, length us, event | category | flops | bytes accessed | tf_op | source)
XLA Modules:
  0.0 135.3 jit_solution(17759099353566622100)
XLA Ops:
  0.0 134.5 %shard_map.136 = bf16[128,2048]{1,0:T(8,128)(2,1)S(1)} custom-call(bf16[128,2048]{1,0:T(8,128)(2,1)} %stream.1, f32[1,2048]{1,0:T(1,128)} %bitcast.9, f32[1,2048]{1,0:T(1,128)} %bitcast.10, bf16[448,128]{1,0:T(8,128)(2,1)} %bitcast.7, bf16[448,128]{1,0:T(8,128)(2,1)} %bitcast.8, bf16[448,128]{1,0:T(8,128)(2,1)} %p_down.1, f32[1,2048]{1,0:T(1,128)} %bitcast.11, ...), custom_call_target="tpu_custom_call" | custom-call | tf_op jit(solution)/shard_map/pallas_call | solution.py:498
  134.5 0.8 copy.16

commit v4 on v3

--- a/solution.py
+++ b/solution.py
@@ -36,11 +36,11 @@
 
 
 def kernel(
-    stream, gain_b, gain_a, p_gate, p_lift, p_down, m_gain, m_u, m_v, l_gain, l_shift, spat, s_shift, m_down,
+    stream, h_gain_b, h_gain_a, p_gate, p_lift, p_down, h_gain_m, m_u, m_v, l_gain, l_shift, spat, s_shift, m_down,
     out,
-    wgl, wd, wuv, wmd, rgl, rd, ruv, rmd, msp, sp2, prm,
+    wgl, wd, wuv, wmd, rgl, rd, ruv, rmd, gate_lift, gain_b, gain_a, m_gain, small, msp, sp2, prm,
     xs, po, ps, pc, pr, acc, hid, hid2, gu, lf, res, sto, sti, colm,
-    w_send, w_recv, x_recv, sw_send, sw_recv, ag_send, ag_recv, rs_send, rs_recv, st_send, st_recv,
+    in_sem, w_send, w_recv, x_recv, sw_send, sw_recv, ag_send, ag_recv, rs_send, rs_recv, st_send, st_recv,
 ):
     rep, fs, tp = lax.axis_index("rep"), lax.axis_index("fs"), lax.axis_index("tp")
     x, c = tp // 2, tp % 2
@@ -76,6 +76,30 @@
 
     def start(copy):
         copy.start()
+
+    loads = [
+        pltpu.make_async_copy(src, dst, in_sem.at[i])
+        for i, (src, dst) in enumerate(
+            (
+                (p_down, wd.at[0, zl, y]),
+                (p_gate, gate_lift.at[0]),
+                (p_lift, gate_lift.at[1]),
+                (stream, res),
+                (h_gain_b, gain_b),
+                (m_u, wuv.at[0, zl, y, :, pl.ds(0, 256)]),
+                (m_v, wuv.at[0, zl, y, :, pl.ds(256, 256)]),
+                (m_down, wmd.at[0, zl, y]),
+                (l_gain, small.at[0]),
+                (l_shift, small.at[1]),
+                (s_shift, small.at[2]),
+                (spat, sp2.at[0]),
+                (h_gain_m, m_gain),
+                (h_gain_a, gain_a),
+            )
+        )
+    ]
+    for load in loads:
+        load.start()
 
     def region(w, s, part, phase, pos, sub):
         n = W_ROWS[w] // 2
@@ -131,9 +155,12 @@
             src, dst = block, relays[w].at[part]
         return remote(src, dst, w_send.at[w * 4 + 3], x_recv.at[w * 4 + relayed * 2 + part], x_dirs[part])
 
-    def px(w):
+    def ready(w):
         for part in (0, 1):
             w_wait(w, 0, part, 0, 2)
+
+    def x1(w):
+        for part in (0, 1):
             start(x_copy(w, part, 0))
 
     def xr(w):
@@ -209,57 +236,49 @@
     def ag_wait_left(r):
         ag_d2d(r, pl.ds(0, 128)).wait_recv()
 
-    def ag_relay(r):
-        for ch in range(CH):
+    def ag_relay(r, chunks=range(CH)):
+        for ch in chunks:
             ag_ici(r, ch).wait_recv()
             start(ag_fwd(r, pl.ds(ch * CROWS, CROWS)))
 
     def ag_wait_right(r):
         ag_fwd(r, pl.ds(0, 128)).wait_recv()
 
+    loads[0].wait()
+    pl.semaphore_wait(barrier, len(greeted))
+    p1(DN)
+    loads[1].wait()
+    loads[2].wait()
     wgl[0, zl, y] = jnp.concatenate(
-        [
-            piece
-            for j in range(3)
-            for piece in (p_gate[j * 128 : (j + 1) * 128], p_lift[j * 128 : (j + 1) * 128])
-        ]
-        + [p_gate[384:448], p_lift[384:448]],
+        [gate_lift[half, j * 128 : (j + 1) * 128] for j in range(3) for half in (0, 1)]
+        + [gate_lift[half, 384:448] for half in (0, 1)],
         axis=0,
     ).T
+    p1(GL)
+    for load in loads[3:]:
+        load.wait()
 
     @pl.loop(0, 128 // STEP)
     def _(i):
         rows = pl.ds(i * STEP, STEP)
-        old = stream[rows, :]
-        res[rows, :] = old
-        xs[0, L, 0, rows, :] = normed(old.astype(F32), gain_b)
-
-    wd[0, zl, y] = p_down[...]
-    wuv[0, zl, y] = jnp.concatenate([m_u[...], m_v[...]], axis=1)
-    wmd[0, zl, y] = m_down[...]
-    prm[0] = jnp.concatenate([l_gain[...], l_shift[...], s_shift[...], jnp.zeros((2, 128), F32)], axis=0)
-    sp2[0] = spat[...]
-
-    pl.semaphore_wait(barrier, len(greeted))
-
+        xs[0, L, 0, rows, :] = normed(res[rows, :].astype(F32), gain_b)
+
+    prm[0] = jnp.concatenate([small[0], small[1], small[2], jnp.zeros((2, 128), F32)], axis=0)
     swap_prm = remote(prm.at[0], prm.at[1], sw_send.at[0], sw_recv.at[0], swap_to)
     swap_sp = remote(sp2.at[0], sp2.at[1], sw_send.at[1], sw_recv.at[1], swap_to)
-    p1(GL)
+    for ch in range(CH):
+        ag_send_chunk(0, ch)
     start(swap_prm)
     start(swap_sp)
-    for ch in range(CH):
-        ag_send_chunk(0, ch)
 
     def batch_x(r, b):
         return xs[r, b].reshape(256, 2048)
 
     def up_slot(r, b, s):
-        @pl.loop(0, 3)
-        def _(j):
-            cols = pl.ds(pl.multiple_of(j * 256, 256), 256)
-            o = dot(batch_x(r, b), wgl[s, :, :, :, cols].reshape(2048, 256))
+        o = dot(batch_x(r, b), wgl[s, :, :, :, 0:768].reshape(2048, 768))
+        for j in range(3):
             to = pl.ds(pl.multiple_of(s * 384 + j * 128, 128), 128)
-            hid[b, :, to] = (silu(o[:, :128]) * o[:, 128:]).astype(BF16)
+            hid[b, :, to] = (silu(o[:, j * 256 : j * 256 + 128]) * o[:, j * 256 + 128 : j * 256 + 256]).astype(BF16)
 
     def up_tail(r, b):
         w = jnp.concatenate([wgl[s, :, :, :, 768:896].reshape(2048, 128) for s in (0, 1)], axis=1)
@@ -286,15 +305,10 @@
         return jnp.concatenate([wmd[0, zz, yy], wmd[1, zz, yy]], axis=0)
 
     def down(r, b, half, lhs, columns_of):
-        @pl.loop(0, 4, unroll=2)
-        def _(n):
-            zz, yy = half * 2 + n // 2, (n % 2) * 2
-            rhs = jnp.concatenate([columns_of(zz, yy), columns_of(zz, yy + 1)], axis=1)
-            o = dot(lhs[b], rhs)
-            cols = pl.ds(pl.multiple_of(n * 256, 256), 256)
-            acc[b, half, :, cols] = o[:128]
-            po[r, b, half, :, cols] = o[128:].astype(BF16)
-
+        rhs = jnp.concatenate([columns_of(half * 2 + n // 4, n % 4) for n in range(8)], axis=1)
+        o = dot(lhs[b], rhs)
+        acc[b, half] = o[:128]
+        po[r, b, half] = o[128:].astype(BF16)
         start(rs_d2d(r, b, half))
 
     def rs_right(r, half):
@@ -307,12 +321,16 @@
 
         start(rs_ici(r, half))
 
-    def down_all(r, lhs, columns_of):
+    def down_all(r, lhs, columns_of, between=None):
         down(r, R, 0, lhs, columns_of)
         down(r, R, 1, lhs, columns_of)
         rs_right(r, 0)
+        if between is not None:
+            between()
+            rs_right(r, 1)
         down(r, L, 0, lhs, columns_of)
-        rs_right(r, 1)
+        if between is None:
+            rs_right(r, 1)
         down(r, L, 1, lhs, columns_of)
 
     def rs_left(r, coefficient, gain):
@@ -345,8 +363,9 @@
         @pl.loop(0, 2)
         def _(s):
             to = pl.ds(pl.multiple_of(s * 256, 256), 256)
-            gu[b, :, to] = gelu(dot(batch_x(1, b), wuv[s, :, :, :, 0:256].reshape(2048, 256)))
-            lf[b, :, to] = gelu(dot(batch_x(1, b), wuv[s, :, :, :, 256:512].reshape(2048, 256)))
+            o = dot(batch_x(1, b), wuv[s].reshape(2048, 512))
+            gu[b, :, to] = gelu(o[:, :256])
+            lf[b, :, to] = gelu(o[:, 256:])
 
     lane = lax.broadcasted_iota(jnp.int32, (128, 128), 1)
 
@@ -409,77 +428,78 @@
                     mixed = dot(msp[n], v.astype(BF16)) + colm[:, 8 + n : 9 + n]
                     hid2[b, tok, cols] = (gu[b, tok, cols] * mixed).astype(BF16)
 
+    p2(DN)
     p2(GL)
-    p1(DN)
-    px(GL)
+    p1(UV)
+    ready(DN)
+    p3(DN, 0)
+    ready(GL)
+    x1(GL)
     p3(GL, 0)
-    p2(DN)
-    p1(UV)
-    p4(GL, 0)
-    xr(GL)
-    px(DN)
-    p3(DN, 0)
     p2(UV)
     p1(MD)
+    p4(DN, 0)
+    xr(GL)
+    x1(DN)
+    p4(GL, 0)
+    ready(UV)
+    p2(MD)
     ag_relay(0)
     ag_wait_left(0)
     ag_wait_right(0)
+    p3(GL, 1)
     p5(GL, 0)
 
     @pl.loop(0, 2)
     def _(b):
         up_slot(0, b, 0)
 
-    p4(DN, 0)
-    p3(GL, 1)
     xr(DN)
-    px(UV)
-    p2(MD)
+    x1(UV)
+    ready(MD)
     p4(GL, 1)
     p3(DN, 1)
-    px(MD)
     xr(UV)
+    x1(MD)
     p5(GL, 1)
-
-    @pl.loop(0, 2)
-    def _(b):
-        up_slot(0, b, 1)
-        up_tail(0, b)
-
+    up_slot(0, L, 1)
+    up_tail(0, L)
     p4(DN, 1)
     p3(UV, 0)
+    up_slot(0, R, 1)
+    up_tail(0, R)
     xr(MD)
+    p5(DN, 0)
+    p5(DN, 1)
     p3(UV, 1)
+    down_all(0, hid, wd_cols)
+    p4(UV, 0)
+    p3(MD, 0)
     swap_prm.wait_recv()
     swap_sp.wait_recv()
     causal = lax.broadcasted_iota(jnp.int32, (128, 128), 0) >= lane
     for s in (0, 1):
         for g in (0, 1):
             msp[s * 2 + g] = jnp.where(causal, sp2[s, g].astype(F32), 0.0).astype(BF16)
-    p5(DN, 0)
-    p5(DN, 1)
-    down_all(0, hid, wd_cols)
-    p4(UV, 0)
-    p3(MD, 0)
     rs_left(0, 0.5, m_gain)
     p4(UV, 1)
     p3(MD, 1)
-    ag_relay(1)
+    p4(MD, 0)
+    ag_relay(1, (0,))
     p5(UV, 0)
     p5(UV, 1)
     ag_wait_left(1)
     mixer_up(L)
-    p4(MD, 0)
+    ag_relay(1, (1,))
+    p4(MD, 1)
     ag_wait_right(1)
     mixer_up(R)
     stat_send()
-    p4(MD, 1)
+    p5(MD, 0)
+    p5(MD, 1)
     stat_combine()
     mixer_mid(R)
-    mixer_mid(L)
-    p5(MD, 0)
-    p5(MD, 1)
-    down_all(1, hid2, wmd_cols)
+    down_all(1, hid2, wmd_cols, lambda: mixer_mid(L))
     rs_left(1, 1.0, gain_a)
     ag_wait_left(2)
     up(2, L)
@@ -488,18 +508,16 @@
     up(2, R)
     down_all(2, hid, wd_cols)
     rs_left(2, 0.5, None)
-
     wait_sent()
 
 
 def layer(stream, gain_b, gain_a, p_gate, p_lift, p_down, m_gain, m_u, m_v, l_gain, l_shift, spat, s_shift, m_down):
-    vmem = pl.BlockSpec(memory_space=pltpu.VMEM)
     dma = pltpu.SemaphoreType.DMA
     return pl.pallas_call(
         kernel,
         out_shape=pltpu.VMEM((128, 2048), BF16),
-        in_specs=[vmem] * 14,
-        out_specs=vmem,
+        in_specs=[pl.BlockSpec(memory_space=pl.ANY)] * 14,
+        out_specs=pl.BlockSpec(memory_space=pltpu.VMEM),
         scratch_shapes=[
             pltpu.VMEM((2, 4, 4, 128, 896), BF16),
             pltpu.VMEM((2, 4, 4, 448, 128), BF16),
@@ -509,6 +527,11 @@
             pltpu.VMEM((2, 4, 224, 128), BF16),
             pltpu.VMEM((2, 4, 64, 512), BF16),
             pltpu.VMEM((2, 4, 128, 128), BF16),
+            pltpu.VMEM((2, 448, 128), BF16),
+            pltpu.VMEM((1, 2048), F32),
+            pltpu.VMEM((1, 2048), F32),
+            pltpu.VMEM((1, 2048), F32),
+            pltpu.VMEM((3, 2, 128), F32),
             pltpu.VMEM((4, 128, 128), BF16),
             pltpu.VMEM((2, 2, 128, 128), BF16),
             pltpu.VMEM((2, 8, 128), F32),
@@ -526,6 +549,7 @@
             pltpu.VMEM((2, 8, 128), F32),
             pltpu.VMEM((2, 3, 8, 128), F32),
             pltpu.VMEM((128, 128), F32),
+            dma((14,)),
             dma((16,)), dma((72,)), dma((16,)),
             dma((2,)), dma((2,)),
             dma((6,)), dma((3 * (CH + 2),)),

time: 135 us -> 131 us (0.970)
  Pallas kernels: 134 us -> 130 us
    pallas_call x1, Pallas kernels: 134 us -> 130 us  [layer(): pl.pallas_call(kernel, out_shape=pltpu.VMEM((128, 2048), BF16), in_specs=...]
where the time goes in v4:
time: 131 us
  Pallas kernels  130 us (99%)
    pallas_call x1, Pallas kernels, layer(): pl.pallas_call(kernel, out_shape=pltpu.VMEM((128, 2048), BF16), in_specs=...  130 us

profile of v4, /device:TPU:1, one launch (start us, length us, event | category | flops | bytes accessed | tf_op | source)
XLA Modules:
  0.0 131.0 jit_solution(15037051939094591488)
XLA Ops:
  0.0 130.2 %shard_map.136 = bf16[128,2048]{1,0:T(8,128)(2,1)S(1)} custom-call(bf16[128,2048]{1,0:T(8,128)(2,1)} %stream.1, f32[1,2048]{1,0:T(1,128)} %bitcast.9, f32[1,2048]{1,0:T(1,128)} %bitcast.10, bf16[448,128]{1,0:T(8,128)(2,1)} %bitcast.7, bf16[448,128]{1,0:T(8,128)(2,1)} %bitcast.8, bf16[448,128]{1,0:T(8,128)(2,1)} %p_down.1, f32[1,2048]{1,0:T(1,128)} %bitcast.11, ...), custom_call_target="tpu_custom_call" | custom-call | tf_op jit(solution)/shard_map/pallas_call | solution.py:516
  130.2 0.8 copy.16

commit v5 on v4

--- a/solution.py
+++ b/solution.py
@@ -84,7 +84,8 @@
                 (p_down, wd.at[0, zl, y]),
                 (p_gate, gate_lift.at[0]),
                 (p_lift, gate_lift.at[1]),
-                (stream, res),
+                (stream.at[pl.ds(0, CROWS)], res.at[0]),
+                (stream.at[pl.ds(CROWS, CROWS)], res.at[1]),
                 (h_gain_b, gain_b),
                 (m_u, wuv.at[0, zl, y, :, pl.ds(0, 256)]),
                 (m_v, wuv.at[0, zl, y, :, pl.ds(256, 256)]),
@@ -194,7 +195,7 @@
             drained(ref.at[0, 0:2], w_send.at[w * 4 + 3])
         for r in range(3):
             drained(xs.at[r, 0], ag_send.at[r * 2])
-            drained(xs.at[r, 0, 0], ag_send.at[r * 2 + 1])
+            drained(xs.at[r, 0, :, 0], ag_send.at[r * 2 + 1])
             drained(po.at[r], rs_send.at[r * 2])
             drained(pc.at[r], rs_send.at[r * 2 + 1])
         drained(sti, st_send.at[0])
@@ -202,28 +203,29 @@
         swap_sp.wait_send()
 
     def ag_ici(r, ch):
-        rows = pl.ds(ch * CROWS, CROWS)
         return remote(
-            xs.at[r, L, 0, rows], xs.at[r, R, 0, rows], ag_send.at[r * 2], ag_recv.at[r * (CH + 2) + ch], partner
+            xs.at[r, L, ch, 0], xs.at[r, R, ch, 0], ag_send.at[r * 2], ag_recv.at[r * (2 * CH + 1) + ch], partner
         )
 
-    def ag_d2d(r, rows):
+    def ag_d2d(r, ch):
+        chunk = pl.ds(0, CH) if ch is None else ch
         return remote(
-            xs.at[r, L, 0, rows], xs.at[r, L, 1, rows], ag_send.at[r * 2], ag_recv.at[r * (CH + 2) + CH], sib
+            xs.at[r, L, chunk, 0], xs.at[r, L, chunk, 1], ag_send.at[r * 2], ag_recv.at[r * (2 * CH + 1) + 2 * CH], sib
         )
 
-    def ag_fwd(r, rows):
+    def ag_fwd(r, ch):
         return remote(
-            xs.at[r, R, 0, rows], xs.at[r, R, 1, rows], ag_send.at[r * 2 + 1], ag_recv.at[r * (CH + 2) + CH + 1], sib
+            xs.at[r, R, ch, 0], xs.at[r, R, ch, 1], ag_send.at[r * 2 + 1], ag_recv.at[r * (2 * CH + 1) + CH + ch], sib
         )
 
-    def rs_d2d(r, b, half):
-        return remote(
-            po.at[r, b, half], ps.at[r, b, half], rs_send.at[r * 2], rs_recv.at[r * 4 + (half if b == R else 2)], sib
-        )
-
-    def rs_ici(r, half):
-        return remote(pc.at[r, half], pr.at[r, half], rs_send.at[r * 2 + 1], rs_recv.at[r * 4 + 3], partner)
+    def rs_d2d_right(r, ch):
+        return remote(po.at[r, R, ch], ps.at[r, R, ch], rs_send.at[r * 2], rs_recv.at[r * (2 * CH + 1) + ch], sib)
+
+    def rs_d2d_left(r):
+        return remote(po.at[r, L], ps.at[r, L], rs_send.at[r * 2], rs_recv.at[r * (2 * CH + 1) + 2 * CH], sib)
+
+    def rs_ici(r, ch):
+        return remote(pc.at[r, ch], pr.at[r, ch], rs_send.at[r * 2 + 1], rs_recv.at[r * (2 * CH + 1) + CH + ch], partner)
 
     def normed(rows, gain):
         factor = lax.rsqrt(jnp.mean(rows * rows, axis=1, keepdims=True) + norm_epsilon)
@@ -231,18 +233,17 @@
 
     def ag_send_chunk(r, ch):
         start(ag_ici(r, ch))
-        start(ag_d2d(r, pl.ds(ch * CROWS, CROWS)))
+        start(ag_d2d(r, ch))
 
     def ag_wait_left(r):
-        ag_d2d(r, pl.ds(0, 128)).wait_recv()
-
-    def ag_relay(r, chunks=range(CH)):
-        for ch in chunks:
-            ag_ici(r, ch).wait_recv()
-            start(ag_fwd(r, pl.ds(ch * CROWS, CROWS)))
-
-    def ag_wait_right(r):
-        ag_fwd(r, pl.ds(0, 128)).wait_recv()
+        ag_d2d(r, None).wait_recv()
+
+    def ag_relay(r, ch):
+        ag_ici(r, ch).wait_recv()
+        start(ag_fwd(r, ch))
+
+    def ag_wait_right(r, ch):
+        ag_fwd(r, ch).wait_recv()
 
     loads[0].wait()
     pl.semaphore_wait(barrier, len(greeted))
@@ -258,10 +259,12 @@
     for load in loads[3:]:
         load.wait()
 
-    @pl.loop(0, 128 // STEP)
-    def _(i):
-        rows = pl.ds(i * STEP, STEP)
-        xs[0, L, 0, rows, :] = normed(res[rows, :].astype(F32), gain_b)
+    for ch in range(CH):
+
+        @pl.loop(0, CROWS // STEP)
+        def _(i):
+            rows = pl.ds(i * STEP, STEP)
+            xs[0, L, ch, 0, rows, :] = normed(res[ch, rows, :].astype(F32), gain_b)
 
     prm[0] = jnp.concatenate([small[0], small[1], small[2], jnp.zeros((2, 128), F32)], axis=0)
     swap_prm = remote(prm.at[0], prm.at[1], sw_send.at[0], sw_recv.at[0], swap_to)
@@ -271,30 +274,41 @@
     start(swap_prm)
     start(swap_sp)
 
-    def batch_x(r, b):
-        return xs[r, b].reshape(256, 2048)
-
-    def up_slot(r, b, s):
-        o = dot(batch_x(r, b), wgl[s, :, :, :, 0:768].reshape(2048, 768))
+    def pick(ref, b, ch):
+        return ref[b].reshape(256, ref.shape[-1]) if ch is None else ref[b, ch]
+
+    def put(ref, b, ch, cols, value):
+        if ch is None:
+            for k in range(CH):
+                ref[b, k, :, cols] = value[k * 128 : (k + 1) * 128]
+        else:
+            ref[b, ch, :, cols] = value
+
+    def batch_x(r, b, ch):
+        return xs[r, b].reshape(256, 2048) if ch is None else xs[r, b, ch].reshape(128, 2048)
+
+    def up_slot(r, b, s, ch=None):
+        o = dot(batch_x(r, b, ch), wgl[s, :, :, :, 0:768].reshape(2048, 768))
         for j in range(3):
             to = pl.ds(pl.multiple_of(s * 384 + j * 128, 128), 128)
-            hid[b, :, to] = (silu(o[:, j * 256 : j * 256 + 128]) * o[:, j * 256 + 128 : j * 256 + 256]).astype(BF16)
-
-    def up_tail(r, b):
+            h = silu(o[:, j * 256 : j * 256 + 128]) * o[:, j * 256 + 128 : j * 256 + 256]
+            put(hid, b, ch, to, h.astype(BF16))
+
+    def up_tail(r, b, ch=None):
         w = jnp.concatenate([wgl[s, :, :, :, 768:896].reshape(2048, 128) for s in (0, 1)], axis=1)
-        o = dot(batch_x(r, b), w)
+        o = dot(batch_x(r, b, ch), w)
         t0, t1 = o[:, :128], o[:, 128:]
-        low = lax.broadcasted_iota(jnp.int32, (256, 128), 1) < 64
+        low = lax.broadcasted_iota(jnp.int32, t0.shape, 1) < 64
         gate = jnp.where(low, t0, pltpu.roll(t1, 64, axis=1))
         lift = jnp.where(low, pltpu.roll(t0, 64, axis=1), t1)
-        hid[b, :, 768:896] = (silu(gate) * lift).astype(BF16)
-
-    def up(r, b):
+        put(hid, b, ch, pl.ds(768, 128), (silu(gate) * lift).astype(BF16))
+
+    def up(r, b, ch=None):
         @pl.loop(0, 2)
         def _(s):
-            up_slot(r, b, s)
-
-        up_tail(r, b)
+            up_slot(r, b, s, ch)
+
+        up_tail(r, b, ch)
 
     def wd_cols(zz, yy):
         return jnp.concatenate(
@@ -304,68 +318,65 @@
     def wmd_cols(zz, yy):
         return jnp.concatenate([wmd[0, zz, yy], wmd[1, zz, yy]], axis=0)
 
-    def down(r, b, half, lhs, columns_of):
+    def down(r, b, ch, half, lhs, columns_of):
         rhs = jnp.concatenate([columns_of(half * 2 + n // 4, n % 4) for n in range(8)], axis=1)
-        o = dot(lhs[b], rhs)
-        acc[b, half] = o[:128]
-        po[r, b, half] = o[128:].astype(BF16)
-        start(rs_d2d(r, b, half))
-
-    def rs_right(r, half):
-        rs_d2d(r, R, half).wait_recv()
-
-        @pl.loop(0, 128 // STEP)
+        o = dot(pick(lhs, b, ch), rhs)
+        cols = pl.ds(half * 1024, 1024)
+        for i, k in enumerate(range(CH) if ch is None else (ch,)):
+            acc[b, k, :, cols] = o[i * 128 : i * 128 + 64]
+            po[r, b, k, :, cols] = o[i * 128 + 64 : i * 128 + 128].astype(BF16)
+
+    def down_right(r, ch, lhs, columns_of):
+        for half in (0, 1):
+            down(r, R, ch, half, lhs, columns_of)
+        start(rs_d2d_right(r, ch))
+
+    def rs_right(r, ch):
+        rs_d2d_right(r, ch).wait_recv()
+
+        @pl.loop(0, CROWS // STEP)
         def _(i):
             rows = pl.ds(i * STEP, STEP)
-            pc[r, half, rows, :] = (acc[R, half, rows, :] + ps[r, R, half, rows, :].astype(F32)).astype(BF16)
-
-        start(rs_ici(r, half))
-
-    def down_all(r, lhs, columns_of, between=None):
-        down(r, R, 0, lhs, columns_of)
-        down(r, R, 1, lhs, columns_of)
-        rs_right(r, 0)
-        if between is not None:
-            between()
-            rs_right(r, 1)
-        down(r, L, 0, lhs, columns_of)
-        if between is None:
-            rs_right(r, 1)
-        down(r, L, 1, lhs, columns_of)
+            pc[r, ch, rows, :] = (acc[R, ch, rows, :] + ps[r, R, ch, rows, :].astype(F32)).astype(BF16)
+
+        start(rs_ici(r, ch))
+
+    def down_rest(r, lhs, columns_of, first):
+        first()
+        down(r, L, None, 0, lhs, columns_of)
+        rs_right(r, 1)
+        down(r, L, None, 1, lhs, columns_of)
+        start(rs_d2d_left(r))
 
     def rs_left(r, coefficient, gain):
-        remote(po.at[r, L], ps.at[r, L], rs_send.at[r * 2], rs_recv.at[r * 4 + 2], sib).wait_recv()
-        remote(pc.at[r], pr.at[r], rs_send.at[r * 2 + 1], rs_recv.at[r * 4 + 3], partner).wait_recv()
+        rs_d2d_left(r).wait_recv()
         for ch in range(CH):
+            rs_ici(r, ch).wait_recv()
 
             @pl.loop(0, CROWS // STEP)
             def _(i):
-                rows = pl.ds(ch * CROWS + i * STEP, STEP)
-                delta = jnp.concatenate(
-                    [
-                        acc[L, half, rows, :] + ps[r, L, half, rows, :].astype(F32) + pr[r, half, rows, :].astype(F32)
-                        for half in (0, 1)
-                    ],
-                    axis=1,
-                )
-                new = (res[rows, :].astype(F32) + coefficient * delta).astype(BF16)
+                rows = pl.ds(i * STEP, STEP)
+                delta = acc[L, ch, rows, :] + ps[r, L, ch, rows, :].astype(F32) + pr[r, ch, rows, :].astype(F32)
+                new = (res[ch, rows, :].astype(F32) + coefficient * delta).astype(BF16)
                 if gain is None:
-                    out[rows, :] = new
+                    out[pl.ds(ch * CROWS + i * STEP, STEP), :] = new
                 else:
-                    res[rows, :] = new
-                    xs[r + 1, L, 0, rows, :] = normed(new.astype(F32), gain)
-
-            rows = pl.ds(ch * CROWS, CROWS)
+                    res[ch, rows, :] = new
+                    xs[r + 1, L, ch, 0, rows, :] = normed(new.astype(F32), gain)
+
             if gain is not None:
                 ag_send_chunk(r + 1, ch)
 
-    def mixer_up(b):
+    def mixer_up(b, ch=None):
         @pl.loop(0, 2)
         def _(s):
             to = pl.ds(pl.multiple_of(s * 256, 256), 256)
-            o = dot(batch_x(1, b), wuv[s].reshape(2048, 512))
-            gu[b, :, to] = gelu(o[:, :256])
-            lf[b, :, to] = gelu(o[:, 256:])
+            o = dot(batch_x(1, b, ch), wuv[s].reshape(2048, 512))
+            put(gu, b, ch, to, gelu(o[:, :256]))
+            put(lf, b, ch, to, gelu(o[:, 256:]))
+
+    def tokens(ref, b, q, cols):
+        return jnp.concatenate([ref[b, k, q * 64 : q * 64 + 64, cols] for k in range(CH)], axis=0)
 
     lane = lax.broadcasted_iota(jnp.int32, (128, 128), 1)
 
@@ -373,7 +384,7 @@
         table = jnp.zeros((128, 128), F32)
         for q in (0, 1):
             for b in (0, 1):
-                v = lf[b, q * 128 : (q + 1) * 128, :]
+                v = tokens(lf, b, q, slice(None))
                 mean = jnp.mean(v, axis=1, keepdims=True)
                 dev2 = jnp.sum(jnp.square(v - mean), axis=1, keepdims=True)
                 table = jnp.where(lane == q * 8 + b * 2, mean, table)
@@ -419,14 +430,15 @@
         for q in (0, 1):
             k = (q * 2 + b) * 2
             centre, factor = colm[:, k : k + 1], colm[:, k + 1 : k + 2]
-            tok = pl.ds(q * 128, 128)
             for s in (0, 1):
                 for g in (0, 1):
                     n = s * 2 + g
                     cols = pl.ds(n * 128, 128)
-                    v = (lf[b, tok, cols] - centre) * factor * prm[s, g : g + 1] + prm[s, 2 + g : 3 + g]
+                    v = (tokens(lf, b, q, cols) - centre) * factor * prm[s, g : g + 1] + prm[s, 2 + g : 3 + g]
                     mixed = dot(msp[n], v.astype(BF16)) + colm[:, 8 + n : 9 + n]
-                    hid2[b, tok, cols] = (gu[b, tok, cols] * mixed).astype(BF16)
+                    gated = (tokens(gu, b, q, cols) * mixed).astype(BF16)
+                    for k in range(CH):
+                        hid2[b, k, q * 64 : q * 64 + 64, cols] = gated[k * 64 : k * 64 + 64]
 
     p2(DN)
     p2(GL)
@@ -444,9 +456,11 @@
     p4(GL, 0)
     ready(UV)
     p2(MD)
-    ag_relay(0)
+    ag_relay(0, 0)
+    ag_relay(0, 1)
     ag_wait_left(0)
-    ag_wait_right(0)
+    ag_wait_right(0, 0)
+    ag_wait_right(0, 1)
     p3(GL, 1)
     p5(GL, 0)
 
@@ -472,7 +486,9 @@
     p5(DN, 0)
     p5(DN, 1)
     p3(UV, 1)
-    down_all(0, hid, wd_cols)
+    down_right(0, 0, hid, wd_cols)
+    down_right(0, 1, hid, wd_cols)
+    down_rest(0, hid, wd_cols, lambda: rs_right(0, 0))
     p4(UV, 0)
     p3(MD, 0)
     swap_prm.wait_recv()
@@ -485,28 +501,39 @@
     p4(UV, 1)
     p3(MD, 1)
     p4(MD, 0)
-    ag_relay(1, (0,))
+    ag_relay(1, 0)
     p5(UV, 0)
     p5(UV, 1)
     ag_wait_left(1)
     mixer_up(L)
-    ag_relay(1, (1,))
+    ag_wait_right(1, 0)
+    ag_relay(1, 1)
     p4(MD, 1)
-    ag_wait_right(1)
-    mixer_up(R)
+    mixer_up(R, 0)
+    ag_wait_right(1, 1)
+    mixer_up(R, 1)
     stat_send()
     p5(MD, 0)
     p5(MD, 1)
     stat_combine()
     mixer_mid(R)
-    down_all(1, hid2, wmd_cols, lambda: mixer_mid(L))
+    down_right(1, 0, hid2, wmd_cols)
+    down_right(1, 1, hid2, wmd_cols)
+    mixer_mid(L)
+    down_rest(1, hid2, wmd_cols, lambda: rs_right(1, 0))
     rs_left(1, 1.0, gain_a)
     ag_wait_left(2)
     up(2, L)
-    ag_relay(2)
-    ag_wait_right(2)
-    up(2, R)
-    down_all(2, hid, wd_cols)
+    ag_relay(2, 0)
+    ag_wait_right(2, 0)
+    up(2, R, 0)
+    ag_relay(2, 1)
+    down_right(2, 0, hid, wd_cols)
+    ag_wait_right(2, 1)
+    up(2, R, 1)
+    rs_right(2, 0)
+    down_right(2, 1, hid, wd_cols)
+    down_rest(2, hid, wd_cols, lambda: None)
     rs_left(2, 0.5, None)
     wait_sent()
 
@@ -535,25 +562,25 @@
             pltpu.VMEM((4, 128, 128), BF16),
             pltpu.VMEM((2, 2, 128, 128), BF16),
             pltpu.VMEM((2, 8, 128), F32),
-            pltpu.VMEM((3, 2, 2, 128, 2048), BF16),
-            pltpu.VMEM((3, 2, 2, 128, 1024), BF16),
-            pltpu.VMEM((3, 2, 2, 128, 1024), BF16),
-            pltpu.VMEM((3, 2, 128, 1024), BF16),
-            pltpu.VMEM((3, 2, 128, 1024), BF16),
-            pltpu.VMEM((2, 2, 128, 1024), F32),
-            pltpu.VMEM((2, 256, 896), BF16),
-            pltpu.VMEM((2, 256, 512), BF16),
-            pltpu.VMEM((2, 256, 512), F32),
-            pltpu.VMEM((2, 256, 512), F32),
-            pltpu.VMEM((128, 2048), BF16),
+            pltpu.VMEM((3, 2, CH, 2, CROWS, 2048), BF16),
+            pltpu.VMEM((3, 2, CH, CROWS, 2048), BF16),
+            pltpu.VMEM((3, 2, CH, CROWS, 2048), BF16),
+            pltpu.VMEM((3, CH, CROWS, 2048), BF16),
+            pltpu.VMEM((3, CH, CROWS, 2048), BF16),
+            pltpu.VMEM((2, CH, CROWS, 2048), F32),
+            pltpu.VMEM((2, CH, 128, 896), BF16),
+            pltpu.VMEM((2, CH, 128, 512), BF16),
+            pltpu.VMEM((2, CH, 128, 512), F32),
+            pltpu.VMEM((2, CH, 128, 512), F32),
+            pltpu.VMEM((CH, CROWS, 2048), BF16),
             pltpu.VMEM((2, 8, 128), F32),
             pltpu.VMEM((2, 3, 8, 128), F32),
             pltpu.VMEM((128, 128), F32),
-            dma((14,)),
+            dma((15,)),
             dma((16,)), dma((72,)), dma((16,)),
             dma((2,)), dma((2,)),
-            dma((6,)), dma((3 * (CH + 2),)),
-            dma((6,)), dma((12,)),
+            dma((6,)), dma((3 * (2 * CH + 1),)),
+            dma((6,)), dma((3 * (2 * CH + 1),)),
             dma((1,)), dma((1,)),
         ],
         compiler_params=pltpu.CompilerParams(

time: 131 us -> 125 us (0.954)
  Pallas kernels: 130 us -> 125 us
    pallas_call x1, Pallas kernels: 130 us -> 125 us  [layer(): pl.pallas_call(kernel, out_shape=pltpu.VMEM((128, 2048), BF16), in_specs=...]
where the time goes in v5:
time: 125 us
  Pallas kernels  125 us (100%)
    pallas_call x1, Pallas kernels, layer(): pl.pallas_call(kernel, out_shape=pltpu.VMEM((128, 2048), BF16), in_specs=...  125 us

profile of v5, /device:TPU:1, one launch (start us, length us, event | category | flops | bytes accessed | tf_op | source)
XLA Modules:
  0.0 125.4 jit_solution(9843594683906172946)
XLA Ops:
  0.0 124.6 %shard_map.136 = bf16[128,2048]{1,0:T(8,128)(2,1)S(1)} custom-call(bf16[128,2048]{1,0:T(8,128)(2,1)} %stream.1, f32[1,2048]{1,0:T(1,128)} %bitcast.9, f32[1,2048]{1,0:T(1,128)} %bitcast.10, bf16[448,128]{1,0:T(8,128)(2,1)} %bitcast.7, bf16[448,128]{1,0:T(8,128)(2,1)} %bitcast.8, bf16[448,128]{1,0:T(8,128)(2,1)} %p_down.1, f32[1,2048]{1,0:T(1,128)} %bitcast.11, ...), custom_call_target="tpu_custom_call" | custom-call | tf_op jit(solution)/shard_map/pallas_call | solution.py:543
  124.6 0.8 copy.16

commit v6 on v5

--- a/solution.py
+++ b/solution.py
@@ -304,10 +304,8 @@
         put(hid, b, ch, pl.ds(768, 128), (silu(gate) * lift).astype(BF16))
 
     def up(r, b, ch=None):
-        @pl.loop(0, 2)
-        def _(s):
+        for s in (0, 1):
             up_slot(r, b, s, ch)
-
         up_tail(r, b, ch)
 
     def wd_cols(zz, yy):
@@ -348,7 +346,7 @@
         down(r, L, None, 1, lhs, columns_of)
         start(rs_d2d_left(r))
 
-    def rs_left(r, coefficient, gain):
+    def rs_left(r, coefficient, gain, between=None):
         rs_d2d_left(r).wait_recv()
         for ch in range(CH):
             rs_ici(r, ch).wait_recv()
@@ -366,11 +364,12 @@
 
             if gain is not None:
                 ag_send_chunk(r + 1, ch)
+            if between is not None and ch == 0:
+                between()
 
     def mixer_up(b, ch=None):
-        @pl.loop(0, 2)
-        def _(s):
-            to = pl.ds(pl.multiple_of(s * 256, 256), 256)
+        for s in (0, 1):
+            to = pl.ds(s * 256, 256)
             o = dot(batch_x(1, b, ch), wuv[s].reshape(2048, 512))
             put(gu, b, ch, to, gelu(o[:, :256]))
             put(lf, b, ch, to, gelu(o[:, 256:]))
@@ -441,15 +440,15 @@
                         hid2[b, k, q * 64 : q * 64 + 64, cols] = gated[k * 64 : k * 64 + 64]
 
     p2(DN)
+    p1(UV)
     p2(GL)
-    p1(UV)
+    p1(MD)
     ready(DN)
     p3(DN, 0)
     ready(GL)
     x1(GL)
     p3(GL, 0)
     p2(UV)
-    p1(MD)
     p4(DN, 0)
     xr(GL)
     x1(DN)
@@ -497,17 +496,20 @@
     for s in (0, 1):
         for g in (0, 1):
             msp[s * 2 + g] = jnp.where(causal, sp2[s, g].astype(F32), 0.0).astype(BF16)
-    rs_left(0, 0.5, m_gain)
-    p4(UV, 1)
-    p3(MD, 1)
+
+    def weights_between():
+        p4(UV, 1)
+        p3(MD, 1)
+
+    rs_left(0, 0.5, m_gain, weights_between)
     p4(MD, 0)
     ag_relay(1, 0)
     p5(UV, 0)
     p5(UV, 1)
+    ag_relay(1, 1)
     ag_wait_left(1)
     mixer_up(L)
     ag_wait_right(1, 0)
-    ag_relay(1, 1)
     p4(MD, 1)
     mixer_up(R, 0)
     ag_wait_right(1, 1)
@@ -523,11 +525,15 @@
     down_rest(1, hid2, wmd_cols, lambda: rs_right(1, 0))
     rs_left(1, 1.0, gain_a)
     ag_wait_left(2)
-    up(2, L)
+    up_slot(2, L, 0)
     ag_relay(2, 0)
+    up_slot(2, L, 1)
+    up_tail(2, L)
     ag_wait_right(2, 0)
-    up(2, R, 0)
+    up_slot(2, R, 0, 0)
     ag_relay(2, 1)
+    up_slot(2, R, 1, 0)
+    up_tail(2, R, 0)
     down_right(2, 0, hid, wd_cols)
     ag_wait_right(2, 1)
     up(2, R, 1)

time: 125 us -> 123 us (0.984)
  Pallas kernels: 125 us -> 122 us
    pallas_call x1, Pallas kernels: 125 us -> 122 us  [layer(): pl.pallas_call(kernel, out_shape=pltpu.VMEM((128, 2048), BF16), in_specs=...]
where the time goes in v6:
time: 123 us
  Pallas kernels  122 us (99%)
    pallas_call x1, Pallas kernels, layer(): pl.pallas_call(kernel, out_shape=pltpu.VMEM((128, 2048), BF16), in_specs=...  122 us

profile of v6, /device:TPU:1, one launch (start us, length us, event | category | flops | bytes accessed | tf_op | source)
XLA Modules:
  0.0 123.3 jit_solution(15686082080400429810)
XLA Ops:
  0.0 122.5 %shard_map.136 = bf16[128,2048]{1,0:T(8,128)(2,1)S(1)} custom-call(bf16[128,2048]{1,0:T(8,128)(2,1)} %stream.1, f32[1,2048]{1,0:T(1,128)} %bitcast.9, f32[1,2048]{1,0:T(1,128)} %bitcast.10, bf16[448,128]{1,0:T(8,128)(2,1)} %bitcast.7, bf16[448,128]{1,0:T(8,128)(2,1)} %bitcast.8, bf16[448,128]{1,0:T(8,128)(2,1)} %p_down.1, f32[1,2048]{1,0:T(1,128)} %bitcast.11, ...), custom_call_target="tpu_custom_call" | custom-call | tf_op jit(solution)/shard_map/pallas_call | solution.py:549
  122.5 0.8 copy.16

commit v7 on v6

--- a/solution.py
+++ b/solution.py
@@ -489,7 +489,6 @@
     down_right(0, 1, hid, wd_cols)
     down_rest(0, hid, wd_cols, lambda: rs_right(0, 0))
     p4(UV, 0)
-    p3(MD, 0)
     swap_prm.wait_recv()
     swap_sp.wait_recv()
     causal = lax.broadcasted_iota(jnp.int32, (128, 128), 0) >= lane
@@ -499,6 +498,7 @@
 
     def weights_between():
         p4(UV, 1)
+        p3(MD, 0)
         p3(MD, 1)
 
     rs_left(0, 0.5, m_gain, weights_between)
@@ -510,8 +510,8 @@
     ag_wait_left(1)
     mixer_up(L)
     ag_wait_right(1, 0)
+    mixer_up(R, 0)
     p4(MD, 1)
-    mixer_up(R, 0)
     ag_wait_right(1, 1)
     mixer_up(R, 1)
     stat_send()

time: 123 us -> 123 us (level)
  no operation moved by 1% of the time
where the time goes in v7:
time: 123 us
  Pallas kernels  122 us (99%)
    pallas_call x1, Pallas kernels, layer(): pl.pallas_call(kernel, out_shape=pltpu.VMEM((128, 2048), BF16), in_specs=...  122 us

profile of v7, /device:TPU:1, one launch (start us, length us, event | category | flops | bytes accessed | tf_op | source)
XLA Modules:
  0.0 122.8 jit_solution(2912908746227393403)
XLA Ops:
  0.0 122.0 %shard_map.136 = bf16[128,2048]{1,0:T(8,128)(2,1)S(1)} custom-call(bf16[128,2048]{1,0:T(8,128)(2,1)} %stream.1, f32[1,2048]{1,0:T(1,128)} %bitcast.9, f32[1,2048]{1,0:T(1,128)} %bitcast.10, bf16[448,128]{1,0:T(8,128)(2,1)} %bitcast.7, bf16[448,128]{1,0:T(8,128)(2,1)} %bitcast.8, bf16[448,128]{1,0:T(8,128)(2,1)} %p_down.1, f32[1,2048]{1,0:T(1,128)} %bitcast.11, ...), custom_call_target="tpu_custom_call" | custom-call | tf_op jit(solution)/shard_map/pallas_call | solution.py:549
  122.0 0.8 copy.16

commit v8 on v7

--- a/solution.py
+++ b/solution.py
@@ -439,10 +439,10 @@
                     for k in range(CH):
                         hid2[b, k, q * 64 : q * 64 + 64, cols] = gated[k * 64 : k * 64 + 64]
 
+    p1(MD)
     p2(DN)
     p1(UV)
     p2(GL)
-    p1(MD)
     ready(DN)
     p3(DN, 0)
     ready(GL)
@@ -503,6 +503,10 @@
 
     rs_left(0, 0.5, m_gain, weights_between)
     p4(MD, 0)
+    def between_right():
+        rs_right(1, 0)
+        mixer_mid(L)
+
     ag_relay(1, 0)
     p5(UV, 0)
     p5(UV, 1)
@@ -521,8 +525,7 @@
     mixer_mid(R)
     down_right(1, 0, hid2, wmd_cols)
     down_right(1, 1, hid2, wmd_cols)
-    mixer_mid(L)
-    down_rest(1, hid2, wmd_cols, lambda: rs_right(1, 0))
+    down_rest(1, hid2, wmd_cols, between_right)
     rs_left(1, 1.0, gain_a)
     ag_wait_left(2)
     up_slot(2, L, 0)

time: 123 us -> 123 us (level)
  no operation moved by 1% of the time
where the time goes in v8:
time: 123 us
  Pallas kernels  122 us (99%)
    pallas_call x1, Pallas kernels, layer(): pl.pallas_call(kernel, out_shape=pltpu.VMEM((128, 2048), BF16), in_specs=...  122 us

profile of v8, /device:TPU:1, one launch (start us, length us, event | category | flops | bytes accessed | tf_op | source)
XLA Modules:
  0.0 122.7 jit_solution(3159896070651098399)
XLA Ops:
  0.0 121.9 %shard_map.136 = bf16[128,2048]{1,0:T(8,128)(2,1)S(1)} custom-call(bf16[128,2048]{1,0:T(8,128)(2,1)} %stream.1, f32[1,2048]{1,0:T(1,128)} %bitcast.9, f32[1,2048]{1,0:T(1,128)} %bitcast.10, bf16[448,128]{1,0:T(8,128)(2,1)} %bitcast.7, bf16[448,128]{1,0:T(8,128)(2,1)} %bitcast.8, bf16[448,128]{1,0:T(8,128)(2,1)} %p_down.1, f32[1,2048]{1,0:T(1,128)} %bitcast.11, ...), custom_call_target="tpu_custom_call" | custom-call | tf_op jit(solution)/shard_map/pallas_call | solution.py:552
  121.9 0.8 copy.16
